TPU v7x, 256 devices: a whole 4x4x8 slice. The times are simulated.
256 devices in a mesh: sp: 32 (over z, y), dp: 8 (over x, core).
Axes of the slice: x: 4, y: 4, z: 8, core: 2. Of those that a mesh axis runs over, the one named last changes fastest.
Arguments:
- queries: bfloat16 [32768, 6144], P(('dp', 'sp')), may hold values from -360 to 360
- latent: bfloat16 [32768, 1024], P(('dp', 'sp')), may hold values from -6 to 6
- rope_key: bfloat16 [32768, 64], P(('dp', 'sp')), may hold values from -6 to 6
- latent_gain: float32 [1024], replicated, may hold values from 0.1 to 1.9
- kv_weight: bfloat16 [1024, 8192], P(None, 'dp'), may hold values from -0.1875 to 0.1875
- gate: bfloat16 [32768, 4096], P(('dp', 'sp')), may hold values from -6 to 6
- out_gain: float32 [4096], replicated, may hold values from 0.1 to 1.9
Outputs:
- attended: bfloat16 [32768, 4096], P(('dp', 'sp'))
All inputs are finite; a program needn't handle non-finite values.
Results may differ from a plain program's by a relative error of at most 0.007.
Values may be sent and summed in bfloat16 or wider, within the bound.
No kernel may reach another device: no remote copies, remote signals or barrier semaphores. Data moves between devices by JAX's collectives and lax.ppermute only.
A program may use at most 128 MiB of HBM per device.

v0:
```python
import jax
import jax.numpy as jnp
from jax import lax
from jax.sharding import PartitionSpec as P

HEADS = 32
NOPE = 128
ROPE = 64
VDIM = 128


EPS = 1e-06
THETA = 10000.0


def in_order(blocks, dim):
    blocks = jnp.moveaxis(blocks, 0, dim)
    shape = blocks.shape
    return blocks.reshape(*shape[:dim], shape[dim] * shape[dim + 1], *shape[dim + 2 :])


def copy_for_each(value, axis):
    length = lax.axis_size(axis)
    return lax.all_to_all(
        jnp.broadcast_to(value[None], (length, *value.shape)), axis, 0, 0, tiled=True
    )


def gathered_copies(value, axis, dim):
    return in_order(copy_for_each(value, axis), dim)


def rotary(values, position):
    half_width = values.shape[-1] // 2
    inverse = THETA ** (-jnp.arange(half_width, dtype=jnp.float32) / half_width)
    angles = position.astype(jnp.float32)[:, None] * inverse[None, :]
    if values.ndim == 3:
        angles = angles[:, None, :]
    cosine = jnp.cos(angles)
    sine_part = jnp.sin(angles)
    front_half = values[..., :half_width].astype(jnp.float32)
    back_half = values[..., half_width:].astype(jnp.float32)
    turned = jnp.concatenate(
        [front_half * cosine - back_half * sine_part, back_half * cosine + front_half * sine_part],
        axis=-1,
    )
    return turned.astype(jnp.bfloat16)


def attend(query_block, keys_plain, keys_rotated, values):
    scores = jnp.einsum(
        "qhd,khd->hqk", query_block[..., :NOPE], keys_plain, preferred_element_type=jnp.float32
    )
    scores = scores + jnp.einsum(
        "qhr,kr->hqk", query_block[..., NOPE:], keys_rotated, preferred_element_type=jnp.float32
    )
    scores = scores * (NOPE + ROPE) ** (-0.5)
    row_max = jnp.max(scores, axis=-1, keepdims=True)
    raised = jnp.exp(scores - row_max)
    weights = (raised / jnp.sum(raised, axis=-1, keepdims=True)).astype(jnp.bfloat16)
    result = jnp.einsum("hqk,khd->qhd", weights, values, preferred_element_type=jnp.float32)
    return result.astype(jnp.bfloat16)


def per_device(queries, latent, rope_key, latent_gain, kv_weight, gate, out_gain):
    own_tokens = queries.shape[0]
    groups = lax.axis_size("sp")
    seq_len = own_tokens * groups
    offset = lax.axis_index("sp") * own_tokens
    position = offset + jnp.arange(own_tokens, dtype=jnp.int32)
    widened = latent.astype(jnp.float32)
    normed = (
        widened * lax.rsqrt(jnp.mean(widened * widened, axis=-1, keepdims=True) + EPS) * latent_gain
    ).astype(jnp.bfloat16)
    keyval = jnp.dot(
        normed,
        lax.all_gather(kv_weight, "dp", axis=1, tiled=True),
        preferred_element_type=jnp.float32,
    ).astype(jnp.bfloat16)
    head_queries = queries.reshape(own_tokens, HEADS, NOPE + ROPE)
    head_queries = jnp.concatenate(
        [head_queries[..., :NOPE], rotary(head_queries[..., NOPE:], position)], axis=-1
    )
    head_queries = head_queries.reshape(own_tokens, HEADS * (NOPE + ROPE))
    rotated_all = gathered_copies(rotary(rope_key, position), "sp", 0)
    query_all, kv_all = (
        lax.all_to_all(head_queries, "sp", split_axis=1, concat_axis=0, tiled=True),
        lax.all_to_all(keyval, "sp", split_axis=1, concat_axis=0, tiled=True),
    )
    local_heads = HEADS // groups
    rows_all = query_all.shape[0]
    seq_count = rows_all // seq_len
    block_rows = min(512, seq_len)
    block_count = seq_len // block_rows

    def one_sequence(operands):
        query_seq, kv_seq, rope_seq = operands
        keys_plain = kv_seq[..., :NOPE]
        values = kv_seq[..., NOPE:]
        blocks = query_seq.reshape(block_count, block_rows, local_heads, NOPE + ROPE)
        result = lax.map(
            lambda piece_rows: attend(piece_rows, keys_plain, rope_seq, values), blocks
        )
        return result.reshape(seq_len, local_heads * VDIM)

    heads_out = lax.map(
        one_sequence,
        (
            query_all.reshape(seq_count, seq_len, local_heads, NOPE + ROPE),
            kv_all.reshape(seq_count, seq_len, local_heads, NOPE + VDIM),
            rotated_all.reshape(seq_count, seq_len, ROPE),
        ),
    )
    heads_out = heads_out.reshape(rows_all, local_heads * VDIM)
    token_rows = lax.all_to_all(heads_out, "sp", split_axis=0, concat_axis=1, tiled=True)
    gated_rows = token_rows.astype(jnp.float32) * jax.nn.silu(gate.astype(jnp.float32))
    scale_rows = lax.rsqrt(jnp.mean(gated_rows * gated_rows, axis=-1, keepdims=True) + EPS)
    return (gated_rows * scale_rows * out_gain).astype(jnp.bfloat16)


def solution(mesh):
    return jax.shard_map(
        per_device,
        mesh=mesh,
        in_specs=(
            P(("dp", "sp"), None),
            P(("dp", "sp"), None),
            P(("dp", "sp"), None),
            P(),
            P(None, "dp"),
            P(("dp", "sp"), None),
            P(),
        ),
        out_specs=P(("dp", "sp"), None),
        check_vma=False,
    )
```

profile of v0, /device:TPU:8, one launch (start us, length us, event | category | flops | bytes accessed | tf_op | source)
XLA Modules:
  0.0 278.0 jit_solution(5976931859334378445)
XLA Ops:
  8.4 11.7 %all-to-all-start.2 = ((bf16[32,128,64]{1,2,0:T(8,128)(2,1)}), bf16[32,128,64]{1,2,0:T(8,128)(2,1)S(1)}, u32[]{:S(2)}, u32[]{:S(2)}) async-start(bf16[32,128,64]{1,2,0:T(8,128)(2,1)} %broadcast_in_dim.7), calls=%async_computation.2 | async-start | bytes 1048576 | tf_op jit(solution)/shard_map/all_to_all | solution.py:24
  20.1 1.9 copy.26
  22.3 1.3 pad_maximum_fusion
  23.6 13.3 %all-to-all-done.2 = bf16[32,128,64]{1,2,0:T(8,128)(2,1)S(1)} async-done(((bf16[32,128,64]{1,2,0:T(8,128)(2,1)}), bf16[32,128,64]{1,2,0:T(8,128)(2,1)S(1)}, u32[]{:S(2)}, u32[]{:S(2)}) %all-to-all-start.2) | async-done | bytes 524320 | tf_op jit(solution)/shard_map/all_to_all | solution.py:24
  36.9 5.6 %all-to-all-start = ((bf16[128,32,192]{0,2,1:T(8,128)(2,1)}), bf16[128,32,192]{0,2,1:T(8,128)(2,1)S(1)}, u32[]{:S(2)}, u32[]{:S(2)}) async-start(bf16[128,32,192]{0,2,1:T(8,128)(2,1)} %pad_maximum_fusion), calls=%async_computation | async-start | bytes 3145728 | tf_op jit(solution)/shard_map/all_to_all | solution.py:87
  42.6 56.9 %all-gather.2.cloned.1.call-done = bf16[1024,8192]{1,0:T(8,128)(2,1)} async-done(((bf16[1024,1024]{1,0:T(8,128)(2,1)}), bf16[1024,8192]{1,0:T(8,128)(2,1)}) %all-gather.2.cloned.1.call-update) | async-done | bytes 16777232 | tf_op jit(solution)/shard_map/all_gather | solution.py:77
  99.5 8.2 %convolution_convert_fusion = bf16[128,8192]{1,0:T(8,128)(2,1)S(1)} fusion(bf16[1024,8192]{1,0:T(8,128)(2,1)} %all-gather.2.cloned.1.call-done, bf16[128,1024]{1,0:T(8,128)(2,1)S(1)} %copy-done.3, f32[1024]{0:T(1024)S(1)} %copy-done.8, f32[128]{0:T(128)S(1)} %add_rsqrt_fusion.1), kind=kOutput, calls=%fused_computation.16 | convolution fusion | flops 2149056512 | bytes 19141120 | tf_op jit(solution)/shard_map/dot_general | solution.py:75
  107.7 1.6 copy.39
  110.5 10.2 %all-to-all-start.1 = ((bf16[128,32,256]{2,0,1:T(8,128)(2,1)}), bf16[128,32,256]{2,0,1:T(8,128)(2,1)S(1)}, u32[]{:S(2)}, u32[]{:S(2)}) async-start(bf16[128,32,256]{2,0,1:T(8,128)(2,1)} %bitcast.86), calls=%async_computation.1 | async-start | bytes 4194304 | tf_op jit(solution)/shard_map/all_to_all | solution.py:88
  120.6 1.5 copy.35
  122.2 3.6 %copy.27 = bf16[32,128,192]{1,0,2:T(8,128)(2,1)} copy(bf16[32,128,192]{1,2,0:T(8,128)(2,1)} %bitcast.88) | data formatting | bytes 3145728 | tf_op jit(solution)/shard_map/all_to_all | solution.py:87
  125.7 3.7 %reshape.157 = bf16[8,512,1,192]{1,0,3,2:T(8,128)(2,1)} reshape(bf16[32,128,192]{1,0,2:T(8,128)(2,1)} %copy.27) | data formatting | bytes 3145728 | tf_op jit(solution)/shard_map/while/body/eval_jaxpr/reshape | solution.py:100
  129.5 3.1 %copy.30 = bf16[8,512,1,192]{1,3,2,0:T(8,128)(2,1)} copy(bf16[8,512,1,192]{1,0,3,2:T(8,128)(2,1)} %reshape.157) | data formatting | bytes 3145728 | tf_op jit(solution)/shard_map/while/body/eval_jaxpr/while | solution.py:101
  132.5 37.7 %all-to-all-done.1 = bf16[128,32,256]{2,0,1:T(8,128)(2,1)S(1)} async-done(((bf16[128,32,256]{2,0,1:T(8,128)(2,1)}), bf16[128,32,256]{2,0,1:T(8,128)(2,1)S(1)}, u32[]{:S(2)}, u32[]{:S(2)}) %all-to-all-start.1) | async-done | bytes 2097184 | tf_op jit(solution)/shard_map/all_to_all | solution.py:88
  170.2 1.3 copy-done
  171.6 2.7 fusion.35
  174.3 57.8 %while.17 = (s32[]{:T(128)}, bf16[8,512,1,128]{3,1,2,0:T(8,128)(2,1)S(1)}, bf16[8,512,1,192]{1,3,2,0:T(8,128)(2,1)}, bf16[4096,1,128]{2,0,1:T(8,128)(2,1)S(1)}, ...) while((s32[]{:T(128)}, bf16[8,512,1,128]{3,1,2,0:T(8,128)(2,1)S(1)}, ...), condition=%wide.region_4.5_spmd, body=%wide.region_1.4_spmd.sunk | while | flops 1359019008 | bytes 50014328 | solution.py:101
  175.3 1.3 fusion.50
  176.5 1.4 fusion.51
  178.0 1.3 fusion.52
  179.3 2.2 fusion.53
  182.5 1.3 fusion.50
  183.8 1.4 fusion.51
  185.2 1.3 fusion.52
  186.5 2.2 fusion.53
  189.7 1.3 fusion.50
  191.0 1.4 fusion.51
  192.4 1.3 fusion.52
  193.7 2.2 fusion.53
  196.9 1.3 fusion.50
  198.2 1.4 fusion.51
  199.7 1.3 fusion.52
  200.9 2.2 fusion.53
  204.2 1.3 fusion.50
  205.4 1.4 fusion.51
  208.2 2.2 fusion.53
  211.4 1.3 fusion.50
  212.7 1.4 fusion.51
  215.4 2.2 fusion.53
  218.6 1.3 fusion.50
  219.9 1.4 fusion.51
  222.6 2.2 fusion.53
  225.8 1.3 fusion.50
  227.1 1.4 fusion.51
  229.8 2.2 fusion.53
  233.1 6.3 %all-to-all-start.3 = ((bf16[32,128,128]{2,1,0:T(8,128)(2,1)}), bf16[32,128,128]{2,1,0:T(8,128)(2,1)S(1)}, u32[]{:S(2)}, u32[]{:S(2)}) async-start(bf16[32,128,128]{2,1,0:T(8,128)(2,1)} %bitcast.91), calls=%async_computation.3 | async-start | bytes 2097152 | tf_op jit(solution)/shard_map/all_to_all | solution.py:115
  240.1 27.4 %all-to-all-done.3 = bf16[32,128,128]{2,1,0:T(8,128)(2,1)S(1)} async-done(((bf16[32,128,128]{2,1,0:T(8,128)(2,1)}), bf16[32,128,128]{2,1,0:T(8,128)(2,1)S(1)}, u32[]{:S(2)}, u32[]{:S(2)}) %all-to-all-start.3) | async-done | bytes 1048608 | tf_op jit(solution)/shard_map/all_to_all | solution.py:115
  269.8 1.3 copy.34
  (65 shorter events, 19.9 us)
Async XLA Ops:
  6.5 0.8 copy-start.10
  6.5 93.0 %all-gather.2.cloned.1.call-start = ((), (), s32[]{:S(2)}) async-start(), calls=%async_computation.4 | async-start | bytes 18874368 | tf_op jit(solution)/shard_map/all_gather | solution.py:77
  8.4 28.5 %all-to-all-start.2 = ((bf16[32,128,64]{1,2,0:T(8,128)(2,1)}), bf16[32,128,64]{1,2,0:T(8,128)(2,1)S(1)}, u32[]{:S(2)}, u32[]{:S(2)}) async-start(bf16[32,128,64]{1,2,0:T(8,128)(2,1)} %broadcast_in_dim.7), calls=%async_computation.2 | async-start | bytes 1048576 | tf_op jit(solution)/shard_map/all_to_all | solution.py:24
  23.6 18.9 %copy-start.3 = (bf16[128,1024]{1,0:T(8,128)(2,1)S(1)}, bf16[128,1024]{1,0:T(8,128)(2,1)}, u32[]{:S(2)}) copy-start(bf16[128,1024]{1,0:T(8,128)(2,1)} %param.10) | copy-start | bytes 786436
  23.6 75.9 %copy-start.8 = (f32[1024]{0:T(1024)S(1)}, f32[1024]{0:T(1024)}, u32[]{:S(2)}) copy-start(f32[1024]{0:T(1024)} %param.12) | copy-start | bytes 12292
  36.9 70.8 %copy-start.2 = (bf16[32,128,64]{1,2,0:T(8,128)(2,1)}, bf16[32,128,64]{1,2,0:T(8,128)(2,1)S(1)}, u32[]{:S(2)}) copy-start(bf16[32,128,64]{1,2,0:T(8,128)(2,1)S(1)} %all-to-all-done.2) | copy-start | bytes 1572868
  36.9 72.4 %all-to-all-start = ((bf16[128,32,192]{0,2,1:T(8,128)(2,1)}), bf16[128,32,192]{0,2,1:T(8,128)(2,1)S(1)}, u32[]{:S(2)}, u32[]{:S(2)}) async-start(bf16[128,32,192]{0,2,1:T(8,128)(2,1)} %pad_maximum_fusion), calls=%async_computation | async-start | bytes 3145728 | tf_op jit(solution)/shard_map/all_to_all | solution.py:87
  109.3 1.2 copy-start.1
  110.5 59.8 %all-to-all-start.1 = ((bf16[128,32,256]{2,0,1:T(8,128)(2,1)}), bf16[128,32,256]{2,0,1:T(8,128)(2,1)S(1)}, u32[]{:S(2)}, u32[]{:S(2)}) async-start(bf16[128,32,256]{2,0,1:T(8,128)(2,1)} %bitcast.86), calls=%async_computation.1 | async-start | bytes 4194304 | tf_op jit(solution)/shard_map/all_to_all | solution.py:88
  170.2 1.3 copy-start
  171.6 2.7 copy-start.5
  178.0 1.3 copy-start.7
  185.2 1.3 copy-start.7
  192.4 1.3 copy-start.7
  199.7 1.3 copy-start.7
  206.9 1.3 copy-start.7
  214.1 1.3 copy-start.7
  221.3 1.3 copy-start.7
  228.6 1.3 copy-start.7
  232.1 1.0 copy-start.6
  232.1 7.3 %copy-start.4 = (bf16[128,4096]{1,0:T(8,128)(2,1)S(1)}, bf16[128,4096]{1,0:T(8,128)(2,1)}, u32[]{:S(2)}) copy-start(bf16[128,4096]{1,0:T(8,128)(2,1)} %param.14) | copy-start | bytes 3145732
  233.1 34.4 %all-to-all-start.3 = ((bf16[32,128,128]{2,1,0:T(8,128)(2,1)}), bf16[32,128,128]{2,1,0:T(8,128)(2,1)S(1)}, u32[]{:S(2)}, u32[]{:S(2)}) async-start(bf16[32,128,128]{2,1,0:T(8,128)(2,1)} %bitcast.91), calls=%async_computation.3 | async-start | bytes 2097152 | tf_op jit(solution)/shard_map/all_to_all | solution.py:115
  240.1 28.8 %copy-start.9 = (f32[4096]{0:T(1024)S(1)}, f32[4096]{0:T(1024)}, u32[]{:S(2)}) copy-start(f32[4096]{0:T(1024)} %param.15) | copy-start | bytes 49156
Sparse Core Ops, SparseCore 0:
  9.2 90.2 all-gather.1
where the time goes:
time: 279 us; the launch traced here: 278 us
  waiting for transfers between devices  136 us (49%)
  matrix products  47.9 us (17%)
  starting transfers between devices  33.8 us (12%)
  local copies, waits for them, and re-layouts  32.8 us (12%)
  other arithmetic  13.6 us (5%)
  between operations  13.6 us (5%)
    all_gather x1, waiting for transfers between devices, per_device(): lax.all_gather(kv_weight, 'dp', axis=1, tiled=True)  56.9 us
    all_to_all x1, waiting for transfers between devices, per_device(): lax.all_to_all(keyval, 'sp', split_axis=1, concat_axis=0, tiled=True)  37.7 us
    all_to_all x1, waiting for transfers between devices, per_device(): lax.all_to_all(heads_out, 'sp', split_axis=0, concat_axis=1, tiled=True)  27.4 us
    dot_general x8, matrix products, attend(): jnp.einsum('hqk,khd->qhd', weights, values, preferred_element_type=jnp.fl...  18 us
    all_to_all x1, waiting for transfers between devices, copy_for_each(): lax.all_to_all(jnp.broadcast_to(value[None], (length, *value.shape)), axi...  13.3 us
    all_to_all x1, starting transfers between devices, copy_for_each(): lax.all_to_all(jnp.broadcast_to(value[None], (length, *value.shape)), axi...  11.7 us
    dot_general x8, matrix products, attend(): jnp.einsum('qhr,kr->hqk', query_block[..., NOPE:], keys_rotated, preferre...  11.4 us
    dot_general x8, matrix products, attend(): jnp.einsum('qhd,khd->hqk', query_block[..., :NOPE], keys_plain, preferred...  10.3 us
  transfers between devices with their start and end apart: 5, of which 4 were waited for; matrix products, arithmetic and copies ran while one was open for 10% of the time, Pallas kernels for 0%

commit v1 on v0

v1 whole, which is shorter than its diff:
```python
import functools
import math

import jax
import jax.numpy as jnp
from jax import lax
from jax.experimental import pallas as pl
from jax.experimental.pallas import tpu as pltpu
from jax.sharding import Mesh
from jax.sharding import PartitionSpec as P

HEADS = 32
NOPE = 128
ROPE = 64
VDIM = 128
RANK = 1024
GROUPS = 8
PER = HEADS // GROUPS
OWN = 128
QCOLS = PER * (NOPE + ROPE)
WIDE = RANK + 2 * ROPE

EPS = 1e-06
THETA = 10000.0
SCALE2 = math.log2(math.e) / math.sqrt(NOPE + ROPE)
F32 = jnp.float32
BF16 = jnp.bfloat16

Z = ("zh", "zl")
DP = ("x", "core")
EVERY = ("zh", "zl", "y", "x", "core")


def turned(pair, cosine, signed_sine):
    u = pair.astype(F32)
    first = lax.broadcasted_iota(jnp.int32, u.shape, 1) % ROPE < ROPE // 2
    partner = jnp.where(first, pltpu.roll(u, 128 - ROPE // 2, 1), pltpu.roll(u, ROPE // 2, 1))
    return (u * cosine + partner * signed_sine).astype(BF16)


def latent_kernel(latent_ref, key_ref, gain_ref, cos_ref, sin_ref, sent_ref):
    wide = latent_ref[...].astype(F32)
    mean = jnp.mean(wide * wide, axis=-1, keepdims=True)
    sent_ref[:, :RANK] = (wide * lax.rsqrt(mean + EPS) * gain_ref[...]).astype(BF16)
    key = key_ref[...]
    sent_ref[:, RANK:] = turned(jnp.concatenate([key, key], axis=1), cos_ref[...], sin_ref[...])


def query_kernel(q_ref, cos_ref, sin_ref, sent_ref):
    cosine, signed_sine = cos_ref[...], sin_ref[...]
    for pair in range(HEADS // 2):
        group, local = pair // (PER // 2), pair % (PER // 2)
        a, b, c = (q_ref[:, 384 * pair + 128 * i : 384 * pair + 128 * (i + 1)] for i in range(3))
        sent_ref[group, :, 256 * local : 256 * local + 128] = a
        sent_ref[group, :, 256 * local + 128 : 256 * local + 256] = jnp.concatenate(
            [b[:, 64:], c[:, :64]], axis=1
        )
        rope = jnp.concatenate([b[:, :64], c[:, 64:]], axis=1)
        base = PER * NOPE + 128 * local
        sent_ref[group, :, base : base + 128] = turned(rope, cosine, signed_sine)


def small_call(kernel, shape, flops, moved):
    return pl.pallas_call(
        kernel,
        out_shape=jax.ShapeDtypeStruct(shape, BF16),
        cost_estimate=pl.CostEstimate(flops=flops, bytes_accessed=moved, transcendentals=0),
    )


def attention_kernel(sizes, bq, bk, q_ref, *refs):
    pieces, (w_ref, o_ref, kext, vt, acc, m_ref, s_ref) = refs[: len(sizes)], refs[len(sizes) :]
    seq = kext.shape[0]
    h = pl.program_id(0)
    lane = lax.broadcasted_iota(jnp.int32, (1, 128), 1)
    keep = (lane >= ROPE) == (h % 2 == 1)

    @pl.when(h == 0)
    def _():
        row = lax.broadcasted_iota(jnp.int32, (16, seq), 0)
        vt[VDIM:, :] = jnp.where(row == 0, 1.0, 0.0).astype(BF16)

    start = 0
    for size, piece in zip(sizes, pieces):
        rows = pl.ds(start, size)
        kv = jnp.dot(piece[:, :RANK], w_ref[...], preferred_element_type=F32)
        kext[rows, :NOPE] = kv[:, :NOPE].astype(BF16)
        rotated = piece[:, RANK:]
        kext[rows, NOPE:] = jnp.where(keep, rotated, jnp.zeros_like(rotated))
        vt[:VDIM, rows] = kv[:, NOPE:].T.astype(BF16)
        start += size

    blocks = seq // bk
    plain = pl.ds(pl.multiple_of(h * NOPE, 128), 128)
    rope = pl.ds(pl.multiple_of(PER * NOPE + (h // 2) * 128, 128), 128)

    def query_block(qb, carry):
        sources = pl.ds(qb * (bq // OWN), bq // OWN)
        q = jnp.concatenate(
            [q_ref[sources, :, plain].reshape(bq, 128), q_ref[sources, :, rope].reshape(bq, 128)],
            axis=1,
        )

        def score(kb):
            rows = pl.ds(pl.multiple_of(kb * bk, bk), bk)
            return lax.dot_general(
                kext[rows, :], q, (((1,), (1,)), ((), ())), preferred_element_type=F32
            )

        m_ref[...] = jnp.full_like(m_ref, -jnp.inf)
        acc[...] = jnp.zeros_like(acc)
        s_ref[0] = score(0)

        def step(kb, slot):
            s_ref[1 - slot] = score(jnp.minimum(kb + 1, blocks - 1))
            s = s_ref[slot]
            m_old = m_ref[0:1, :]
            m_new = jnp.maximum(m_old, jnp.max(s, axis=0, keepdims=True))
            p = jnp.exp2((s - m_new) * SCALE2).astype(BF16)
            shrink = jnp.exp2((m_old - m_new) * SCALE2)
            rows = pl.ds(pl.multiple_of(kb * bk, bk), bk)
            acc[...] = acc[...] * shrink + jnp.dot(vt[:, rows], p, preferred_element_type=F32)
            m_ref[0:1, :] = m_new

        def two(i, inner):
            step(2 * i, 0)
            step(2 * i + 1, 1)
            return inner

        lax.fori_loop(0, blocks // 2, two, 0)
        out = (acc[:VDIM, :] / acc[VDIM : VDIM + 1, :]).T.astype(BF16)
        o_ref[sources, :, :] = out.reshape(bq // OWN, OWN, VDIM)
        return carry

    lax.fori_loop(0, GROUPS * OWN // bq, query_block, 0)


def attention(queries, pieces, weight, bq=512, bk=1024):
    sizes = tuple(p.shape[0] for p in pieces)
    seq = sum(sizes)
    rows = GROUPS * OWN
    flops = 2 * PER * (seq * RANK * 256 + rows * seq * 400)
    return pl.pallas_call(
        functools.partial(attention_kernel, sizes, bq, bk),
        grid=(PER,),
        in_specs=[pl.BlockSpec((GROUPS, OWN, QCOLS), lambda h: (0, 0, 0))]
        + [pl.BlockSpec((s, WIDE), lambda h: (0, 0)) for s in sizes]
        + [pl.BlockSpec((RANK, NOPE + VDIM), lambda h: (0, h))],
        out_specs=pl.BlockSpec((GROUPS, OWN, VDIM), lambda h: (0, 0, h)),
        out_shape=jax.ShapeDtypeStruct((GROUPS, OWN, PER * VDIM), BF16),
        scratch_shapes=[
            pltpu.VMEM((seq, 256), BF16),
            pltpu.VMEM((VDIM + 16, seq), BF16),
            pltpu.VMEM((VDIM + 16, bq), F32),
            pltpu.VMEM((8, bq), F32),
            pltpu.VMEM((2, bk, bq), F32),
        ],
        cost_estimate=pl.CostEstimate(
            flops=flops, bytes_accessed=14 * 2**20, transcendentals=PER * rows * seq
        ),
        compiler_params=pltpu.CompilerParams(
            dimension_semantics=("arbitrary",), vmem_limit_bytes=56 * 2**20
        ),
    )(queries, *pieces, weight)


def gate_kernel(heads_ref, gate_ref, gain_ref, out_ref, gated):
    total = jnp.zeros((OWN, 1), F32)
    width = PER * VDIM
    for group in range(GROUPS):
        columns = slice(group * width, (group + 1) * width)
        v = gate_ref[:, columns].astype(F32)
        part = heads_ref[group].astype(F32) * (v * jax.nn.sigmoid(v))
        gated[:, columns] = part
        total += jnp.sum(part * part, axis=-1, keepdims=True)
    scale = lax.rsqrt(total / (HEADS * VDIM) + EPS)
    for group in range(GROUPS):
        columns = slice(group * width, (group + 1) * width)
        out_ref[:, columns] = (gated[:, columns] * scale * gain_ref[:, columns]).astype(BF16)


def gate_and_norm(heads, gate, gain):
    return pl.pallas_call(
        gate_kernel,
        out_shape=jax.ShapeDtypeStruct((OWN, HEADS * VDIM), BF16),
        scratch_shapes=[pltpu.VMEM((OWN, HEADS * VDIM), F32)],
        cost_estimate=pl.CostEstimate(flops=10**7, bytes_accessed=3 * 2**20, transcendentals=0),
    )(heads, gate, gain)


def shifted(value, axis, by):
    length = lax.axis_size(axis)
    return lax.ppermute(value, axis, [(i, (i + by) % length) for i in range(length)])


def ring(value, axis):
    length = lax.axis_size(axis)
    ahead, behind, blocks = value, value, [value]
    for _ in range(length // 2 - 1):
        ahead, behind = shifted(ahead, axis, 1), shifted(behind, axis, -1)
        blocks += [ahead, behind]
    half = value.shape[0] // 2
    return blocks + [shifted(ahead[:half], axis, 1), shifted(behind[half:], axis, -1)]


def along(move, mesh_shape):
    zh_n, zl_n, y_n, x_n, core_n = mesh_shape
    pairs = []
    for zh in range(zh_n):
        for zl in range(zl_n):
            for y in range(y_n):
                group = zl * y_n + y
                column = ((zh * zl_n + zl) * y_n + y) * x_n * core_n
                for source, target in move(group // core_n, group % core_n, x_n):
                    pairs.append((column + source, column + target))
    return pairs


def shard_of_group(weight, mesh_shape):
    def one_way(by):
        return along(lambda x, c, n: [(x * 2 + c, (x + by) % n * 2 + c)], mesh_shape)

    def far(by):
        return along(
            lambda x, c, n: [((x + by) % n * 2 + c, (x + 2) % n * 2 + c)], mesh_shape
        )

    swap = along(lambda x, c, n: [(i * 2 + c, i * 2 + 1 - c) for i in range(n)], mesh_shape)
    group = lax.axis_index("zl") * lax.axis_size("y") + lax.axis_index("y")
    mine = lax.axis_index(DP) == group
    half = weight.shape[0] // 2
    right = lax.ppermute(weight, EVERY, one_way(1))
    left = lax.ppermute(weight, EVERY, one_way(-1))
    opposite = jnp.concatenate(
        [
            lax.ppermute(right[:half], EVERY, far(1)),
            lax.ppermute(left[half:], EVERY, far(-1)),
        ]
    )
    held = jnp.where(mine, weight, right + left + opposite)
    other = lax.ppermute(held, EVERY, swap)
    return jnp.where(lax.axis_index("core") == group % 2, held, other)


def per_device(mesh_shape, queries, latent, rope_key, latent_gain, kv_weight, gate, out_gain):
    block = lax.axis_index(("zh", "zl", "y"))
    position = block * OWN + jnp.arange(OWN, dtype=jnp.int32)
    half = ROPE // 2
    inverse = THETA ** (-jnp.arange(half, dtype=F32) / half)
    angles = position.astype(F32)[:, None] * inverse[None, :]
    cosine, sine = jnp.cos(angles), jnp.sin(angles)
    cosine = jnp.concatenate([cosine] * 4, axis=1)
    sine = jnp.concatenate([-sine, sine] * 2, axis=1)

    weight = shard_of_group(kv_weight, mesh_shape)
    sent = small_call(latent_kernel, (OWN, WIDE), 10**6, 2**20)(
        latent, rope_key, latent_gain[None, :], cosine, sine
    )
    head_queries = small_call(query_kernel, (GROUPS, OWN, QCOLS), 10**7, 3 * 2**20)(
        queries, cosine, sine
    )
    head_queries = lax.all_to_all(head_queries, ("zl", "y"), 0, 0, tiled=True)

    along_z = jnp.concatenate(ring(sent[: OWN // 2], Z))
    along_y = jnp.concatenate(ring(sent[OWN // 2 :], "y"))
    pieces = ring(along_z, "y") + ring(along_y, Z)

    heads_out = attention(head_queries, pieces, weight)
    heads_out = lax.all_to_all(heads_out, ("zl", "y"), 0, 0, tiled=True)
    return gate_and_norm(heads_out, gate, out_gain[None, :])


def solution(mesh):
    x_n, z_n, y_n = mesh.shape["dp"] // 2, 8, mesh.shape["sp"] // 8
    mesh_shape = (z_n // 2, 2, y_n, x_n, 2)
    named = Mesh(mesh.devices.reshape(mesh_shape), EVERY)
    tokens = P(("x", "core", "zh", "zl", "y"), None)
    return jax.shard_map(
        functools.partial(per_device, mesh_shape),
        mesh=named,
        in_specs=(tokens, tokens, tokens, P(), P(None, DP), tokens, P()),
        out_specs=tokens,
        check_vma=False,
    )
```

time: 279 us -> 194 us (0.70)
  waiting for transfers between devices: 136 us -> 46.7 us
  Pallas kernels: 0 us -> 48.3 us
  matrix products: 47.9 us -> 0 us
  starting transfers between devices: 33.8 us -> 61.4 us
  local copies, waits for them, and re-layouts: 32.8 us -> 8.66 us
  blocking collectives: 0 us -> 19.5 us
  between operations: 13.6 us -> 0.32 us
  other arithmetic: 13.6 us -> 8.61 us
    all_to_all x4 -> x1, waiting for transfers between devices: 78.4 us -> 0.01 us  [per_device(): head_queries = lax.all_to_all(head_queries, ('zl', 'y'), 0, 0, tiled=True)]
    all_gather x1 -> x0, waiting for transfers between devices: 56.9 us -> none  [per_device(): lax.all_gather(kv_weight, 'dp', axis=1, tiled=True)]
    ppermute x0 -> x29, starting transfers between devices: none -> 53 us  [the longest x24 47.3 us: shifted(): lax.ppermute(value, axis, [(i, (i + by) % length) for i in range(length)])]
    pallas_call x0 -> x4, Pallas kernels: none -> 48.3 us  [the longest x1 39.7 us: attention(): pl.pallas_call(functools.partial(attention_kernel, sizes, bq, bk), grid=(...]
    dot_general x25 -> x0, matrix products: 47.9 us -> none  [the longest x8 18 us: attend(): jnp.einsum('hqk,khd->qhd', weights, values, preferred_element_type=jnp.fl...]
    ppermute x0 -> x29, waiting for transfers between devices: none -> 46.7 us  [the longest x24 46.7 us: shifted(): lax.ppermute(value, axis, [(i, (i + by) % length) for i in range(length)])]
    all_to_all x4 -> x1, starting transfers between devices: 33.8 us -> 8.34 us  [per_device(): head_queries = lax.all_to_all(head_queries, ('zl', 'y'), 0, 0, tiled=True)]
    all_to_all x0 -> x1, blocking collectives: none -> 19.5 us  [per_device(): heads_out = lax.all_to_all(heads_out, ('zl', 'y'), 0, 0, tiled=True)]
  transfers between devices with their start and end apart: 5 -> 30, of which waited for: 4 -> 10; matrix products, arithmetic and copies ran while one was open for 10% -> 8% of each run, Pallas kernels for 0% -> 3%
where the time goes in v1:
time: 194 us; the launch traced here: 193 us
  starting transfers between devices  61.4 us (32%)
  Pallas kernels  48.3 us (25%)
  waiting for transfers between devices  46.7 us (24%)
  blocking collectives  19.5 us (10%)
  local copies, waits for them, and re-layouts  8.66 us (4%)
  other arithmetic  8.61 us (4%)
    ppermute x24, starting transfers between devices, shifted(): lax.ppermute(value, axis, [(i, (i + by) % length) for i in range(length)])  47.3 us
    ppermute x24, waiting for transfers between devices, shifted(): lax.ppermute(value, axis, [(i, (i + by) % length) for i in range(length)])  46.7 us
    pallas_call x1, Pallas kernels, attention(): pl.pallas_call(functools.partial(attention_kernel, sizes, bq, bk), grid=(...  39.7 us
    all_to_all x1, blocking collectives, per_device(): heads_out = lax.all_to_all(heads_out, ('zl', 'y'), 0, 0, tiled=True)  19.5 us
    all_to_all x1, starting transfers between devices, per_device(): head_queries = lax.all_to_all(head_queries, ('zl', 'y'), 0, 0, tiled=True)  8.34 us
    select_n x1, other arithmetic, shard_of_group(): held = jnp.where(mine, weight, right + left + opposite)  4.29 us
  transfers between devices with their start and end apart: 30, of which 10 were waited for; matrix products, arithmetic and copies ran while one was open for 8% of the time, Pallas kernels for 3%

profile of v1, /device:TPU:8, one launch (start us, length us, event | category | flops | bytes accessed | tf_op | source)
XLA Modules:
  0.0 193.5 jit_solution(8856469818656908570)
XLA Ops:
  0.0 0.8 collective-permute-start.24
  0.8 2.0 %collective-permute-start.25 = (bf16[1024,1024]{1,0:T(8,128)(2,1)}, bf16[1024,1024]{1,0:T(8,128)(2,1)}, u32[]{:S(2)}, u32[]{:S(2)}) collective-permute-start(bf16[1024,1024]{1,0:T(8,128)(2,1)} %param.11), channel_id=1, source_target_pairs={{0,6},{9,15},{18,16},{27,25},{36,34},{45,43},{54,52},{63,61},{64,7... | collective-permute-start | bytes 6291464 | tf_op jit(solution)/shard_map/ppermute | solution.py:233
  2.8 1.4 copy.10.key_ref
  4.6 0.8 pad_maximum_fusion
  5.4 1.9 shard_map.74
  7.3 1.7 fusion.2
  9.0 0.9 collective-permute-start.12
  9.9 3.6 %collective-permute-start.13 = (bf16[64,1152]{1,0:T(8,128)(2,1)S(1)}, bf16[64,1152]{1,0:T(8,128)(2,1)S(1)}, u32[]{:S(2)}, u32[]{:S(2)}) collective-permute-start(bf16[64,1152]{1,0:T(8,128)(2,1)S(1)} %get-tuple-element.5), channel_id=1, source_target_pairs={{0,24},{8,0},{16,8},{24,16},{1,25},{9,1},{17,9},{25,17},{2,26},{10... | collective-permute-start | bytes 442376 | tf_op jit(solution)/shard_map/ppermute | solution.py:193
  13.5 3.3 %shard_map.73 = bf16[8,128,768]{2,1,0:T(8,128)(2,1)} custom-call(bf16[128,6144]{1,0:T(8,128)(2,1)} %q_ref.1, f32[128,128]{1,0:T(8,128)} %get-tuple-element.12.cos_ref, f32[128,128]{1,0:T(8,128)} %get-tuple-element.13.sin_ref), custom_call_target="tpu_custom_call" | custom-call | flops 10000000 | bytes 3145728 | tf_op jit(solution)/shard_map/pallas_call | solution.py:259
  16.7 8.3 %all-to-all-start = ((bf16[8,128,768]{2,1,0:T(8,128)(2,1)}), bf16[8,128,768]{2,1,0:T(8,128)(2,1)}, u32[]{:S(2)}, u32[]{:S(2)}) async-start(bf16[8,128,768]{2,1,0:T(8,128)(2,1)} %shard_map.73), calls=%async_computation | async-start | bytes 3145728 | tf_op jit(solution)/shard_map/all_to_all | solution.py:262
  25.1 5.4 %collective-permute-start.1 = (bf16[64,1152]{1,0:T(8,128)(2,1)S(1)}, bf16[64,1152]{1,0:T(8,128)(2,1)S(1)}, u32[]{:S(2)}, u32[]{:S(2)}) collective-permute-start(bf16[64,1152]{1,0:T(8,128)(2,1)S(1)} %get-tuple-element.8), channel_id=1, source_target_pairs={{0,224},{32,0},{64,32},{96,64},{128,96},{160,128},{192,160},{224,1... | collective-permute-start | bytes 442376 | tf_op jit(solution)/shard_map/ppermute | solution.py:193
  30.5 1.5 collective-permute-start.14
  32.1 0.6 collective-permute-start.15
  32.7 0.7 constant_dynamic-update-slice_fusion.7
  33.5 0.9 collective-permute-start.26
  34.4 1.5 slice.59
  35.9 10.3 %collective-permute-done.1 = bf16[64,1152]{1,0:T(8,128)(2,1)S(1)} collective-permute-done((bf16[64,1152]{1,0:T(8,128)(2,1)S(1)}, bf16[64,1152]{1,0:T(8,128)(2,1)S(1)}, u32[]{:S(2)}, u32[]{:S(2)}) %collective-permute-start.1) | collective-permute-done | bytes 147488 | tf_op jit(solution)/shard_map/ppermute | solution.py:193
  46.2 0.7 collective-permute-start.27
  46.9 2.4 %collective-permute-start.3 = (bf16[64,1152]{1,0:T(8,128)(2,1)S(1)}, bf16[64,1152]{1,0:T(8,128)(2,1)S(1)}, u32[]{:S(2)}, u32[]{:S(2)}) collective-permute-start(bf16[64,1152]{1,0:T(8,128)(2,1)S(1)} %collective-permute-done.1), channel_id=1, source_target_pairs={{0,224},{32,0},{64,32},{96,64},{128,96},{160,128},{192,160},{224,1... | collective-permute-start | bytes 442376 | tf_op jit(solution)/shard_map/ppermute | solution.py:193
  49.5 2.8 %collective-permute-start.4 = (bf16[64,1152]{1,0:T(8,128)(2,1)S(1)}, bf16[64,1152]{1,0:T(8,128)(2,1)S(1)}, u32[]{:S(2)}, u32[]{:S(2)}) collective-permute-start(bf16[64,1152]{1,0:T(8,128)(2,1)S(1)} %collective-permute-done.2), channel_id=1, source_target_pairs={{0,32},{32,64},{64,96},{96,128},{128,160},{160,192},{192,224},{224... | collective-permute-start | bytes 442376 | tf_op jit(solution)/shard_map/ppermute | solution.py:193
  52.2 3.8 %collective-permute-start.5 = (bf16[64,1152]{1,0:T(8,128)(2,1)S(1)}, bf16[64,1152]{1,0:T(8,128)(2,1)S(1)}, u32[]{:S(2)}, u32[]{:S(2)}) collective-permute-start(bf16[64,1152]{1,0:T(8,128)(2,1)S(1)} %collective-permute-done.3), channel_id=1, source_target_pairs={{0,224},{32,0},{64,32},{96,64},{128,96},{160,128},{192,160},{224,1... | collective-permute-start | bytes 442376 | tf_op jit(solution)/shard_map/ppermute | solution.py:193
  56.0 10.3 %collective-permute-done.4 = bf16[64,1152]{1,0:T(8,128)(2,1)S(1)} collective-permute-done((bf16[64,1152]{1,0:T(8,128)(2,1)S(1)}, bf16[64,1152]{1,0:T(8,128)(2,1)S(1)}, u32[]{:S(2)}, u32[]{:S(2)}) %collective-permute-start.4) | collective-permute-done | bytes 147488 | tf_op jit(solution)/shard_map/ppermute | solution.py:193
  66.3 0.6 collective-permute-start.17
  67.0 1.6 collective-permute-start.6
  68.6 1.9 collective-permute-start.7
  70.6 4.3 %fusion = bf16[1024,1024]{1,0:T(8,128)(2,1)S(1)} fusion(bf16[1024,1024]{1,0:T(8,128)(2,1)S(1)} %copy-done.1, bf16[512,1024]{1,0:T(8,128)(2,1)S(1)} %collective-permute-done.27, bf16[512,1024]{1,0:T(8,128)(2,1)S(1)} %collective-permute-done.26, bf16[1024,1024]{1,0:T(8,128)(2,1)} %copy-done, bf16[1024,1024]{1,0:T(8,128)(2,1)} %collective-permute-done.25, pred[]{:T(512)S(6)} %eq.9), kind=kLoop, calls=%fused_computation.1 | loop fusion | flops 9437184 | bytes 10485761 | tf_op jit(solution)/shard_map/jit(_where)/select_n | solution.py:240
  74.9 1.3 collective-permute-start.28
  76.2 3.3 %collective-permute-done.7 = bf16[32,1152]{1,0:T(8,128)(2,1)S(1)} collective-permute-done((bf16[32,1152]{1,0:T(8,128)(2,1)S(1)}, bf16[32,1152]{1,0:T(8,128)(2,1)S(1)}, u32[]{:S(2)}, u32[]{:S(2)}) %collective-permute-start.7) | collective-permute-done | bytes 73760 | tf_op jit(solution)/shard_map/ppermute | solution.py:193
  79.5 1.4 collective-permute-start.8
  80.9 4.4 %collective-permute-start.9 = (bf16[512,1152]{1,0:T(8,128)(2,1)S(1)}, bf16[512,1152]{1,0:T(8,128)(2,1)S(1)}, u32[]{:S(2)}, u32[]{:S(2)}) collective-permute-start(bf16[512,1152]{1,0:T(8,128)(2,1)S(1)} %constant_dynamic-update-slice_fusion.refs_0_), channel_id=1, source_target_pairs={{0,24},{8,0},{16,8},{24,16},{1,25},{9,1},{17,9},{25,17},{2,26},{10... | collective-permute-start | bytes 3538952 | tf_op jit(solution)/shard_map/ppermute | solution.py:193
  85.3 3.2 %collective-permute-start.19 = (bf16[256,1152]{1,0:T(8,128)(2,1)S(1)}, bf16[256,1152]{1,0:T(8,128)(2,1)}, u32[]{:S(2)}, u32[]{:S(2)}) collective-permute-start(bf16[256,1152]{1,0:T(8,128)(2,1)S(1)} %collective-permute-done.17.refs_7_), channel_id=1, source_target_pairs={{0,224},{32,0},{64,32},{96,64},{128,96},{160,128},{192,160},{224,1... | collective-permute-start | bytes 1769480 | tf_op jit(solution)/shard_map/ppermute | solution.py:193
  88.5 10.7 %collective-permute-done.18.refs_8_ = bf16[256,1152]{1,0:T(8,128)(2,1)} collective-permute-done((bf16[256,1152]{1,0:T(8,128)(2,1)S(1)}, bf16[256,1152]{1,0:T(8,128)(2,1)}, u32[]{:S(2)}, u32[]{:S(2)}) %collective-permute-start.18) | collective-permute-done | bytes 589856 | tf_op jit(solution)/shard_map/ppermute | solution.py:193
  99.3 3.2 %collective-permute-start.21 = (bf16[256,1152]{1,0:T(8,128)(2,1)}, bf16[256,1152]{1,0:T(8,128)(2,1)}, u32[]{:S(2)}, u32[]{:S(2)}) collective-permute-start(bf16[256,1152]{1,0:T(8,128)(2,1)} %collective-permute-done.19.refs_9_), channel_id=1, source_target_pairs={{0,224},{32,0},{64,32},{96,64},{128,96},{160,128},{192,160},{224,1... | collective-permute-start | bytes 1769480 | tf_op jit(solution)/shard_map/ppermute | solution.py:193
  102.5 6.5 %collective-permute-done.8.refs_1_ = bf16[512,1152]{1,0:T(8,128)(2,1)S(1)} collective-permute-done((bf16[512,1152]{1,0:T(8,128)(2,1)S(1)}, bf16[512,1152]{1,0:T(8,128)(2,1)S(1)}, u32[]{:S(2)}, u32[]{:S(2)}) %collective-permute-start.8) | collective-permute-done | bytes 1179680 | tf_op jit(solution)/shard_map/ppermute | solution.py:193
  109.1 5.1 %collective-permute-start.10 = (bf16[256,1152]{1,0:T(8,128)(2,1)S(1)}, bf16[256,1152]{1,0:T(8,128)(2,1)}, u32[]{:S(2)}, u32[]{:S(2)}) collective-permute-start(bf16[256,1152]{1,0:T(8,128)(2,1)S(1)} %slice.51), channel_id=1, source_target_pairs={{0,8},{8,16},{16,24},{24,0},{1,9},{9,17},{17,25},{25,1},{2,10},{10... | collective-permute-start | bytes 1769480 | tf_op jit(solution)/shard_map/ppermute | solution.py:193
  114.5 1.0 copy-done.3
  115.6 1.2 collective-permute-start.11
  116.9 1.0 slice.56
  118.0 1.0 slice.57
  119.0 3.5 %collective-permute-start.23 = (bf16[128,1152]{1,0:T(8,128)(2,1)S(1)}, bf16[128,1152]{1,0:T(8,128)(2,1)S(1)}, u32[]{:S(2)}, u32[]{:S(2)}) collective-permute-start(bf16[128,1152]{1,0:T(8,128)(2,1)S(1)} %slice.57), channel_id=1, source_target_pairs={{0,224},{32,0},{64,32},{96,64},{128,96},{160,128},{192,160},{224,1... | collective-permute-start | bytes 884744 | tf_op jit(solution)/shard_map/ppermute | solution.py:193
  122.5 3.2 %broadcast_select_fusion.refs_14_ = bf16[1024,1024]{1,0:T(8,128)(2,1)} fusion(bf16[1024,1024]{1,0:T(8,128)(2,1)S(1)} %fusion, bf16[1024,1024]{1,0:T(8,128)(2,1)} %collective-permute-done.28, pred[]{:T(512)S(6)} %eq.8), kind=kLoop, calls=%fused_computation.2 | loop fusion | flops 1048576 | bytes 6291457 | tf_op jit(solution)/shard_map/jit(_where)/select_n | solution.py:242
  125.6 2.1 %collective-permute-done.22.refs_12_ = bf16[128,1152]{1,0:T(8,128)(2,1)S(1)} collective-permute-done((bf16[128,1152]{1,0:T(8,128)(2,1)S(1)}, bf16[128,1152]{1,0:T(8,128)(2,1)S(1)}, u32[]{:S(2)}, u32[]{:S(2)}) %collective-permute-start.22) | collective-permute-done | bytes 294944 | tf_op jit(solution)/shard_map/ppermute | solution.py:193
  127.7 0.6 collective-permute-done.23.refs_13_
  128.3 0.8 collective-permute-done.10.refs_3_
  129.1 1.7 collective-permute-done.11.refs_4_
  130.8 39.7 %shard_map.75 = bf16[8,128,512]{2,1,0:T(8,128)(2,1)} custom-call(bf16[8,128,768]{2,1,0:T(8,128)(2,1)} %all-to-all-done.q_ref, bf16[512,1152]{1,0:T(8,128)(2,1)} %copy-done.6, bf16[512,1152]{1,0:T(8,128)(2,1)} %copy-done.2, bf16[512,1152]{1,0:T(8,128)(2,1)} %copy-done.3, bf16[256,1152]{1,0:T(8,128)(2,1)} %collective-permute-done.10.refs_3_, ...), custom_call_target="tpu_custom_call" | custom-call | flops 22011707392 | bytes 14680064 | tf_op jit(solution)/shard_map/pallas_call | solution.py:143
  170.6 19.5 %all_to_all.10.heads_ref = bf16[8,128,512]{2,1,0:T(8,128)(2,1)} all-to-all(bf16[8,128,512]{2,1,0:T(8,128)(2,1)} %shard_map.75), channel_id=1, replica_groups=mesh['zh'=4,'zl'=2,'y'=4,'x'=4,'core'=2] {'zl','y'}, dimensions={0} | all-to-all | bytes 2097152 | tf_op jit(solution)/shard_map/all_to_all | solution.py:269
  190.1 3.4 %shard_map.76 = bf16[128,4096]{1,0:T(8,128)(2,1)} custom-call(bf16[8,128,512]{2,1,0:T(8,128)(2,1)} %all_to_all.10.heads_ref, bf16[128,4096]{1,0:T(8,128)(2,1)} %gate_ref.1, f32[1,4096]{1,0:T(1,128)} %bitcast.2), custom_call_target="tpu_custom_call" | custom-call | flops 10000000 | bytes 3145728 | tf_op jit(solution)/shard_map/pallas_call | solution.py:183
  (69 shorter events, 1.3 us)
Async XLA Ops:
  0.0 33.4 %collective-permute-start.24 = (bf16[1024,1024]{1,0:T(8,128)(2,1)}, bf16[1024,1024]{1,0:T(8,128)(2,1)S(1)}, u32[]{:S(2)}, u32[]{:S(2)}) collective-permute-start(bf16[1024,1024]{1,0:T(8,128)(2,1)} %param.11), channel_id=1, source_target_pairs={{0,2},{9,11},{18,20},{27,29},{36,38},{45,47},{54,48},{63,57},{64,6... | collective-permute-start | bytes 6291464 | tf_op jit(solution)/shard_map/ppermute | solution.py:232
  0.8 32.7 %collective-permute-start.25 = (bf16[1024,1024]{1,0:T(8,128)(2,1)}, bf16[1024,1024]{1,0:T(8,128)(2,1)}, u32[]{:S(2)}, u32[]{:S(2)}) collective-permute-start(bf16[1024,1024]{1,0:T(8,128)(2,1)} %param.11), channel_id=1, source_target_pairs={{0,6},{9,15},{18,16},{27,25},{36,34},{45,43},{54,52},{63,61},{64,7... | collective-permute-start | bytes 6291464 | tf_op jit(solution)/shard_map/ppermute | solution.py:233
  9.0 16.1 %collective-permute-start.12 = (bf16[64,1152]{1,0:T(8,128)(2,1)S(1)}, bf16[64,1152]{1,0:T(8,128)(2,1)S(1)}, u32[]{:S(2)}, u32[]{:S(2)}) collective-permute-start(bf16[64,1152]{1,0:T(8,128)(2,1)S(1)} %get-tuple-element.5), channel_id=1, source_target_pairs={{0,8},{8,16},{16,24},{24,0},{1,9},{9,17},{17,25},{25,1},{2,10},{10... | collective-permute-start | bytes 442376 | tf_op jit(solution)/shard_map/ppermute | solution.py:193
  9.9 20.6 %collective-permute-start.13 = (bf16[64,1152]{1,0:T(8,128)(2,1)S(1)}, bf16[64,1152]{1,0:T(8,128)(2,1)S(1)}, u32[]{:S(2)}, u32[]{:S(2)}) collective-permute-start(bf16[64,1152]{1,0:T(8,128)(2,1)S(1)} %get-tuple-element.5), channel_id=1, source_target_pairs={{0,24},{8,0},{16,8},{24,16},{1,25},{9,1},{17,9},{25,17},{2,26},{10... | collective-permute-start | bytes 442376 | tf_op jit(solution)/shard_map/ppermute | solution.py:193
  13.5 18.6 %collective-permute-start = (bf16[64,1152]{1,0:T(8,128)(2,1)S(1)}, bf16[64,1152]{1,0:T(8,128)(2,1)S(1)}, u32[]{:S(2)}, u32[]{:S(2)}) collective-permute-start(bf16[64,1152]{1,0:T(8,128)(2,1)S(1)} %get-tuple-element.8), channel_id=1, source_target_pairs={{0,32},{32,64},{64,96},{96,128},{128,160},{160,192},{192,224},{224... | collective-permute-start | bytes 442376 | tf_op jit(solution)/shard_map/ppermute | solution.py:193
  16.7 114.1 %all-to-all-start = ((bf16[8,128,768]{2,1,0:T(8,128)(2,1)}), bf16[8,128,768]{2,1,0:T(8,128)(2,1)}, u32[]{:S(2)}, u32[]{:S(2)}) async-start(bf16[8,128,768]{2,1,0:T(8,128)(2,1)} %shard_map.73), calls=%async_computation | async-start | bytes 3145728 | tf_op jit(solution)/shard_map/all_to_all | solution.py:262
  25.1 21.1 %collective-permute-start.1 = (bf16[64,1152]{1,0:T(8,128)(2,1)S(1)}, bf16[64,1152]{1,0:T(8,128)(2,1)S(1)}, u32[]{:S(2)}, u32[]{:S(2)}) collective-permute-start(bf16[64,1152]{1,0:T(8,128)(2,1)S(1)} %get-tuple-element.8), channel_id=1, source_target_pairs={{0,224},{32,0},{64,32},{96,64},{128,96},{160,128},{192,160},{224,1... | collective-permute-start | bytes 442376 | tf_op jit(solution)/shard_map/ppermute | solution.py:193
  30.5 16.4 %collective-permute-start.14 = (bf16[32,1152]{1,0:T(8,128)(2,1)S(1)}, bf16[32,1152]{1,0:T(8,128)(2,1)S(1)}, u32[]{:S(2)}, u32[]{:S(2)}) collective-permute-start(bf16[32,1152]{1,0:T(8,128)(2,1)S(1)} %slice.54), channel_id=1, source_target_pairs={{0,8},{8,16},{16,24},{24,0},{1,9},{9,17},{17,25},{25,1},{2,10},{10... | collective-permute-start | bytes 221192 | tf_op jit(solution)/shard_map/ppermute | solution.py:193
  32.1 17.2 %collective-permute-start.15 = (bf16[32,1152]{1,0:T(8,128)(2,1)S(1)}, bf16[32,1152]{1,0:T(8,128)(2,1)S(1)}, u32[]{:S(2)}, u32[]{:S(2)}) collective-permute-start(bf16[32,1152]{1,0:T(8,128)(2,1)S(1)} %slice.55), channel_id=1, source_target_pairs={{0,24},{8,0},{16,8},{24,16},{1,25},{9,1},{17,9},{25,17},{2,26},{10... | collective-permute-start | bytes 221192 | tf_op jit(solution)/shard_map/ppermute | solution.py:193
  33.4 2.4 %copy-start = (bf16[1024,1024]{1,0:T(8,128)(2,1)}, bf16[1024,1024]{1,0:T(8,128)(2,1)S(1)}, u32[]{:S(2)}) copy-start(bf16[1024,1024]{1,0:T(8,128)(2,1)S(1)} %collective-permute-done.24) | copy-start | bytes 6291460
  33.4 16.0 %collective-permute-start.2 = (bf16[64,1152]{1,0:T(8,128)(2,1)S(1)}, bf16[64,1152]{1,0:T(8,128)(2,1)S(1)}, u32[]{:S(2)}, u32[]{:S(2)}) collective-permute-start(bf16[64,1152]{1,0:T(8,128)(2,1)S(1)} %collective-permute-done), channel_id=1, source_target_pairs={{0,32},{32,64},{64,96},{96,128},{128,160},{160,192},{192,224},{224... | collective-permute-start | bytes 442376 | tf_op jit(solution)/shard_map/ppermute | solution.py:193
  33.5 13.4 %copy-start.5 = (bf16[512,1152]{1,0:T(8,128)(2,1)S(1)}, bf16[512,1152]{1,0:T(8,128)(2,1)}, u32[]{:S(2)}) copy-start(bf16[512,1152]{1,0:T(8,128)(2,1)} %constant_dynamic-update-slice_fusion.7) | copy-start | bytes 3538948
  33.5 35.1 %collective-permute-start.26 = (bf16[512,1024]{1,0:T(8,128)(2,1)S(1)}, bf16[512,1024]{1,0:T(8,128)(2,1)S(1)}, u32[]{:S(2)}, u32[]{:S(2)}) collective-permute-start(bf16[512,1024]{1,0:T(8,128)(2,1)S(1)} %slice.58), channel_id=1, source_target_pairs={{2,4},{11,13},{20,22},{29,31},{38,32},{47,41},{48,50},{57,59},{66,... | collective-permute-start | bytes 3145736 | tf_op jit(solution)/shard_map/ppermute | solution.py:236
  34.4 36.2 %copy-start.1 = (bf16[1024,1024]{1,0:T(8,128)(2,1)S(1)}, bf16[1024,1024]{1,0:T(8,128)(2,1)}, u32[]{:S(2)}) copy-start(bf16[1024,1024]{1,0:T(8,128)(2,1)} %param.11) | copy-start | bytes 6291460
  46.2 24.4 %collective-permute-start.27 = (bf16[512,1024]{1,0:T(8,128)(2,1)S(1)}, bf16[512,1024]{1,0:T(8,128)(2,1)S(1)}, u32[]{:S(2)}, u32[]{:S(2)}) collective-permute-start(bf16[512,1024]{1,0:T(8,128)(2,1)S(1)} %slice.59), channel_id=1, source_target_pairs={{6,4},{15,13},{16,22},{25,31},{34,32},{43,41},{52,50},{61,59},{70,... | collective-permute-start | bytes 3145736 | tf_op jit(solution)/shard_map/ppermute | solution.py:237
  46.9 5.3 %collective-permute-start.3 = (bf16[64,1152]{1,0:T(8,128)(2,1)S(1)}, bf16[64,1152]{1,0:T(8,128)(2,1)S(1)}, u32[]{:S(2)}, u32[]{:S(2)}) collective-permute-start(bf16[64,1152]{1,0:T(8,128)(2,1)S(1)} %collective-permute-done.1), channel_id=1, source_target_pairs={{0,224},{32,0},{64,32},{96,64},{128,96},{160,128},{192,160},{224,1... | collective-permute-start | bytes 442376 | tf_op jit(solution)/shard_map/ppermute | solution.py:193
  49.4 25.5 %copy-start.4 = (bf16[256,1152]{1,0:T(8,128)(2,1)}, bf16[256,1152]{1,0:T(8,128)(2,1)S(1)}, u32[]{:S(2)}) copy-start(bf16[256,1152]{1,0:T(8,128)(2,1)S(1)} %constant_dynamic-update-slice_fusion.9.refs_5_) | copy-start | bytes 1769476
  49.4 35.9 %collective-permute-start.16 = (bf16[256,1152]{1,0:T(8,128)(2,1)S(1)}, bf16[256,1152]{1,0:T(8,128)(2,1)S(1)}, u32[]{:S(2)}, u32[]{:S(2)}) collective-permute-start(bf16[256,1152]{1,0:T(8,128)(2,1)S(1)} %constant_dynamic-update-slice_fusion.9.refs_5_), channel_id=1, source_target_pairs={{0,32},{32,64},{64,96},{96,128},{128,160},{160,192},{192,224},{224... | collective-permute-start | bytes 1769480 | tf_op jit(solution)/shard_map/ppermute | solution.py:193
  49.5 16.8 %collective-permute-start.4 = (bf16[64,1152]{1,0:T(8,128)(2,1)S(1)}, bf16[64,1152]{1,0:T(8,128)(2,1)S(1)}, u32[]{:S(2)}, u32[]{:S(2)}) collective-permute-start(bf16[64,1152]{1,0:T(8,128)(2,1)S(1)} %collective-permute-done.2), channel_id=1, source_target_pairs={{0,32},{32,64},{64,96},{96,128},{128,160},{160,192},{192,224},{224... | collective-permute-start | bytes 442376 | tf_op jit(solution)/shard_map/ppermute | solution.py:193
  52.2 14.7 %collective-permute-start.5 = (bf16[64,1152]{1,0:T(8,128)(2,1)S(1)}, bf16[64,1152]{1,0:T(8,128)(2,1)S(1)}, u32[]{:S(2)}, u32[]{:S(2)}) collective-permute-start(bf16[64,1152]{1,0:T(8,128)(2,1)S(1)} %collective-permute-done.3), channel_id=1, source_target_pairs={{0,224},{32,0},{64,32},{96,64},{128,96},{160,128},{192,160},{224,1... | collective-permute-start | bytes 442376 | tf_op jit(solution)/shard_map/ppermute | solution.py:193
  66.3 19.0 %collective-permute-start.17 = (bf16[256,1152]{1,0:T(8,128)(2,1)S(1)}, bf16[256,1152]{1,0:T(8,128)(2,1)S(1)}, u32[]{:S(2)}, u32[]{:S(2)}) collective-permute-start(bf16[256,1152]{1,0:T(8,128)(2,1)S(1)} %constant_dynamic-update-slice_fusion.9.refs_5_), channel_id=1, source_target_pairs={{0,224},{32,0},{64,32},{96,64},{128,96},{160,128},{192,160},{224,1... | collective-permute-start | bytes 1769480 | tf_op jit(solution)/shard_map/ppermute | solution.py:193
  67.0 9.2 %collective-permute-start.6 = (bf16[32,1152]{1,0:T(8,128)(2,1)S(1)}, bf16[32,1152]{1,0:T(8,128)(2,1)S(1)}, u32[]{:S(2)}, u32[]{:S(2)}) collective-permute-start(bf16[32,1152]{1,0:T(8,128)(2,1)S(1)} %slice.49), channel_id=1, source_target_pairs={{0,32},{32,64},{64,96},{96,128},{128,160},{160,192},{192,224},{224... | collective-permute-start | bytes 221192 | tf_op jit(solution)/shard_map/ppermute | solution.py:193
  68.6 10.9 %collective-permute-start.7 = (bf16[32,1152]{1,0:T(8,128)(2,1)S(1)}, bf16[32,1152]{1,0:T(8,128)(2,1)S(1)}, u32[]{:S(2)}, u32[]{:S(2)}) collective-permute-start(bf16[32,1152]{1,0:T(8,128)(2,1)S(1)} %slice.50), channel_id=1, source_target_pairs={{0,224},{32,0},{64,32},{96,64},{128,96},{160,128},{192,160},{224,1... | collective-permute-start | bytes 221192 | tf_op jit(solution)/shard_map/ppermute | solution.py:193
  74.9 47.6 %collective-permute-start.28 = (bf16[1024,1024]{1,0:T(8,128)(2,1)S(1)}, bf16[1024,1024]{1,0:T(8,128)(2,1)}, u32[]{:S(2)}, u32[]{:S(2)}) collective-permute-start(bf16[1024,1024]{1,0:T(8,128)(2,1)S(1)} %fusion), channel_id=1, source_target_pairs={{0,1},{2,3},{4,5},{6,7},{9,8},{11,10},{13,12},{15,14},{16,17},{18,... | collective-permute-start | bytes 6291464 | tf_op jit(solution)/shard_map/ppermute | solution.py:241
  79.5 36.1 %copy-start.6 = (bf16[512,1152]{1,0:T(8,128)(2,1)}, bf16[512,1152]{1,0:T(8,128)(2,1)S(1)}, u32[]{:S(2)}) copy-start(bf16[512,1152]{1,0:T(8,128)(2,1)S(1)} %constant_dynamic-update-slice_fusion.refs_0_) | copy-start | bytes 3538948
  79.5 29.5 %collective-permute-start.8 = (bf16[512,1152]{1,0:T(8,128)(2,1)S(1)}, bf16[512,1152]{1,0:T(8,128)(2,1)S(1)}, u32[]{:S(2)}, u32[]{:S(2)}) collective-permute-start(bf16[512,1152]{1,0:T(8,128)(2,1)S(1)} %constant_dynamic-update-slice_fusion.refs_0_), channel_id=1, source_target_pairs={{0,8},{8,16},{16,24},{24,0},{1,9},{9,17},{17,25},{25,1},{2,10},{10... | collective-permute-start | bytes 3538952 | tf_op jit(solution)/shard_map/ppermute | solution.py:193
  80.9 33.6 %collective-permute-start.9 = (bf16[512,1152]{1,0:T(8,128)(2,1)S(1)}, bf16[512,1152]{1,0:T(8,128)(2,1)S(1)}, u32[]{:S(2)}, u32[]{:S(2)}) collective-permute-start(bf16[512,1152]{1,0:T(8,128)(2,1)S(1)} %constant_dynamic-update-slice_fusion.refs_0_), channel_id=1, source_target_pairs={{0,24},{8,0},{16,8},{24,16},{1,25},{9,1},{17,9},{25,17},{2,26},{10... | collective-permute-start | bytes 3538952 | tf_op jit(solution)/shard_map/ppermute | solution.py:193
  85.3 30.3 %copy-start.7 = (bf16[256,1152]{1,0:T(8,128)(2,1)}, bf16[256,1152]{1,0:T(8,128)(2,1)S(1)}, u32[]{:S(2)}) copy-start(bf16[256,1152]{1,0:T(8,128)(2,1)S(1)} %collective-permute-done.16.refs_6_) | copy-start | bytes 1769476
  85.3 14.0 %collective-permute-start.18 = (bf16[256,1152]{1,0:T(8,128)(2,1)S(1)}, bf16[256,1152]{1,0:T(8,128)(2,1)}, u32[]{:S(2)}, u32[]{:S(2)}) collective-permute-start(bf16[256,1152]{1,0:T(8,128)(2,1)S(1)} %collective-permute-done.16.refs_6_), channel_id=1, source_target_pairs={{0,32},{32,64},{64,96},{96,128},{128,160},{160,192},{192,224},{224... | collective-permute-start | bytes 1769480 | tf_op jit(solution)/shard_map/ppermute | solution.py:193
  85.3 17.2 %copy-start.8 = (bf16[256,1152]{1,0:T(8,128)(2,1)}, bf16[256,1152]{1,0:T(8,128)(2,1)S(1)}, u32[]{:S(2)}) copy-start(bf16[256,1152]{1,0:T(8,128)(2,1)S(1)} %collective-permute-done.17.refs_7_) | copy-start | bytes 1769476
  85.3 14.0 %collective-permute-start.19 = (bf16[256,1152]{1,0:T(8,128)(2,1)S(1)}, bf16[256,1152]{1,0:T(8,128)(2,1)}, u32[]{:S(2)}, u32[]{:S(2)}) collective-permute-start(bf16[256,1152]{1,0:T(8,128)(2,1)S(1)} %collective-permute-done.17.refs_7_), channel_id=1, source_target_pairs={{0,224},{32,0},{64,32},{96,64},{128,96},{160,128},{192,160},{224,1... | collective-permute-start | bytes 1769480 | tf_op jit(solution)/shard_map/ppermute | solution.py:193
  99.3 17.6 %collective-permute-start.20 = (bf16[256,1152]{1,0:T(8,128)(2,1)}, bf16[256,1152]{1,0:T(8,128)(2,1)}, u32[]{:S(2)}, u32[]{:S(2)}) collective-permute-start(bf16[256,1152]{1,0:T(8,128)(2,1)} %collective-permute-done.18.refs_8_), channel_id=1, source_target_pairs={{0,32},{32,64},{64,96},{96,128},{128,160},{160,192},{192,224},{224... | collective-permute-start | bytes 1769480 | tf_op jit(solution)/shard_map/ppermute | solution.py:193
  99.3 18.7 %collective-permute-start.21 = (bf16[256,1152]{1,0:T(8,128)(2,1)}, bf16[256,1152]{1,0:T(8,128)(2,1)}, u32[]{:S(2)}, u32[]{:S(2)}) collective-permute-start(bf16[256,1152]{1,0:T(8,128)(2,1)} %collective-permute-done.19.refs_9_), channel_id=1, source_target_pairs={{0,224},{32,0},{64,32},{96,64},{128,96},{160,128},{192,160},{224,1... | collective-permute-start | bytes 1769480 | tf_op jit(solution)/shard_map/ppermute | solution.py:193
  109.0 6.6 %copy-start.2 = (bf16[512,1152]{1,0:T(8,128)(2,1)}, bf16[512,1152]{1,0:T(8,128)(2,1)S(1)}, u32[]{:S(2)}) copy-start(bf16[512,1152]{1,0:T(8,128)(2,1)S(1)} %collective-permute-done.8.refs_1_) | copy-start | bytes 3538948
  109.1 20.0 %collective-permute-start.10 = (bf16[256,1152]{1,0:T(8,128)(2,1)S(1)}, bf16[256,1152]{1,0:T(8,128)(2,1)}, u32[]{:S(2)}, u32[]{:S(2)}) collective-permute-start(bf16[256,1152]{1,0:T(8,128)(2,1)S(1)} %slice.51), channel_id=1, source_target_pairs={{0,8},{8,16},{16,24},{24,0},{1,9},{9,17},{17,25},{25,1},{2,10},{10... | collective-permute-start | bytes 1769480 | tf_op jit(solution)/shard_map/ppermute | solution.py:193
  114.5 1.0 copy-start.3
  115.6 15.2 %collective-permute-start.11 = (bf16[256,1152]{1,0:T(8,128)(2,1)S(1)}, bf16[256,1152]{1,0:T(8,128)(2,1)}, u32[]{:S(2)}, u32[]{:S(2)}) collective-permute-start(bf16[256,1152]{1,0:T(8,128)(2,1)S(1)} %slice.52), channel_id=1, source_target_pairs={{0,24},{8,0},{16,8},{24,16},{1,25},{9,1},{17,9},{25,17},{2,26},{10... | collective-permute-start | bytes 1769480 | tf_op jit(solution)/shard_map/ppermute | solution.py:193
  117.9 9.8 %collective-permute-start.22 = (bf16[128,1152]{1,0:T(8,128)(2,1)S(1)}, bf16[128,1152]{1,0:T(8,128)(2,1)S(1)}, u32[]{:S(2)}, u32[]{:S(2)}) collective-permute-start(bf16[128,1152]{1,0:T(8,128)(2,1)S(1)} %slice.56), channel_id=1, source_target_pairs={{0,32},{32,64},{64,96},{96,128},{128,160},{160,192},{192,224},{224... | collective-permute-start | bytes 884744 | tf_op jit(solution)/shard_map/ppermute | solution.py:193
  119.0 9.3 %collective-permute-start.23 = (bf16[128,1152]{1,0:T(8,128)(2,1)S(1)}, bf16[128,1152]{1,0:T(8,128)(2,1)S(1)}, u32[]{:S(2)}, u32[]{:S(2)}) collective-permute-start(bf16[128,1152]{1,0:T(8,128)(2,1)S(1)} %slice.57), channel_id=1, source_target_pairs={{0,224},{32,0},{64,32},{96,64},{128,96},{160,128},{192,160},{224,1... | collective-permute-start | bytes 884744 | tf_op jit(solution)/shard_map/ppermute | solution.py:193
  127.7 1.4 copy-start.9
  128.3 0.8 copy-start.10

commit v2 on v1

v2 whole, which is shorter than its diff:
```python
import functools
import math

import jax
import jax.numpy as jnp
from jax import lax
from jax.experimental import pallas as pl
from jax.experimental.pallas import tpu as pltpu
from jax.sharding import Mesh
from jax.sharding import PartitionSpec as P


HEADS = 32
NOPE = 128
ROPE = 64
VDIM = 128
QK = NOPE + ROPE
RANK = 1024
GROUPS = 8
PER = HEADS // GROUPS
OWN = 128
ROWS = GROUPS * OWN
WIDE = RANK + 2 * ROPE

EPS = 1e-06
THETA = 10000.0
SCALE2 = math.log2(math.e) / math.sqrt(QK)
F32 = jnp.float32
BF16 = jnp.bfloat16

Z = ("zh", "zl")
SP = ("zh", "zl", "y")
DP = ("x", "core")
EVERY = ("zh", "zl", "y", "x", "core")


def call(kernel, shape, flops, moved, transcendentals=0, limit=None, **rest):
    return pl.pallas_call(
        kernel,
        out_shape=jax.ShapeDtypeStruct(shape, BF16),
        cost_estimate=pl.CostEstimate(
            flops=flops, bytes_accessed=moved, transcendentals=transcendentals
        ),
        compiler_params=pltpu.CompilerParams(vmem_limit_bytes=limit),
        **rest,
    )


def latent_kernel(latent_ref, key_ref, gain_ref, cos_ref, sin_ref, sent_ref):
    wide = latent_ref[...].astype(F32)
    mean = jnp.mean(wide * wide, axis=-1, keepdims=True)
    sent_ref[:, :RANK] = (wide * lax.rsqrt(mean + EPS) * gain_ref[...]).astype(BF16)
    u1, u2 = key_ref[:, : ROPE // 2].astype(F32), key_ref[:, ROPE // 2 :].astype(F32)
    cosine, sine = cos_ref[...], sin_ref[...]
    turned = [u1 * cosine - u2 * sine, u2 * cosine + u1 * sine]
    turned.append(jnp.zeros((OWN, ROPE), F32))
    sent_ref[:, RANK:] = jnp.concatenate(turned, axis=1).astype(BF16)


def query_kernel(q_ref, cos_ref, sin_ref, sent_ref):
    cosine, sine = cos_ref[...].T, sin_ref[...].T
    for pair in range(HEADS // 2):
        both = jnp.concatenate(
            [q_ref[:, 384 * pair + 128 * i : 384 * pair + 128 * (i + 1)].T for i in range(3)], axis=0
        )
        for side in range(2):
            head = both[QK * side : QK * (side + 1)]
            group, local = divmod(2 * pair + side, PER)
            to = group % (GROUPS // 2), group // (GROUPS // 2), local
            sent_ref[*to, :NOPE] = head[:NOPE]
            u1 = head[NOPE : NOPE + ROPE // 2].astype(F32)
            u2 = head[NOPE + ROPE // 2 :].astype(F32)
            turned = jnp.concatenate([u1 * cosine - u2 * sine, u2 * cosine + u1 * sine], axis=0)
            sent_ref[*to, NOPE:] = turned.astype(BF16)


def attention_kernel(sizes, bq, bk, begins, ends, q_ref, *refs):
    pieces, refs = refs[: len(sizes)], refs[len(sizes) :]
    w_ref, refs = refs[0], refs[1:]
    if not begins:
        acc_in, m_in, refs = refs[0], refs[1], refs[2:]
    (out_ref, refs) = (refs[0], refs[1:]) if ends else (None, refs)
    acc, m_ref, kext, vt, s_ref, q = refs
    keys = kext.shape[0]

    row = lax.broadcasted_iota(jnp.int32, (16, keys), 0)
    vt[VDIM:, :] = jnp.where(row == 0, 1.0, 0.0).astype(BF16)
    start = 0
    for size, piece in zip(sizes, pieces):
        step = min(size, 512)
        for at in range(0, size, step):
            kv = jnp.dot(piece[at : at + step, :RANK], w_ref[...], preferred_element_type=F32)
            rows = slice(start, start + step)
            kext[rows, :NOPE] = kv[:, :NOPE].astype(BF16)
            kext[rows, NOPE:] = piece[at : at + step, RANK:]
            vt[:VDIM, rows] = kv[:, NOPE:].T.astype(BF16)
            start += step
    for source in range(GROUPS):
        q[:QK, source * OWN : (source + 1) * OWN] = q_ref[source, 0]
    q[QK:, :] = jnp.zeros((256 - QK, ROWS), BF16)
    if begins:
        m_ref[...] = jnp.full(m_ref.shape, -jnp.inf, F32)
        acc[...] = jnp.zeros(acc.shape, F32)
    else:
        m_ref[...] = m_in[...]
        acc[...] = acc_in[...]

    blocks = keys // bk
    steps = blocks * (ROWS // bq)

    def score(t):
        rows = pl.ds(pl.multiple_of(lax.rem(t, blocks) * bk, bk), bk)
        columns = pl.ds(pl.multiple_of(lax.div(t, blocks) * bq, bq), bq)
        return jnp.dot(kext[rows, :], q[:, columns], preferred_element_type=F32)

    s_ref[0] = score(0)

    def step(t, slot):
        s_ref[1 - slot] = score(jnp.minimum(t + 1, steps - 1))
        s = s_ref[slot]
        rows = pl.ds(pl.multiple_of(lax.rem(t, blocks) * bk, bk), bk)
        columns = pl.ds(pl.multiple_of(lax.div(t, blocks) * bq, bq), bq)
        m_old = m_ref[0, 0:1, columns]
        m_new = jnp.maximum(m_old, jnp.max(s, axis=0, keepdims=True))
        p = jnp.exp2((s - m_new) * SCALE2).astype(BF16)
        shrink = jnp.exp2((m_old - m_new) * SCALE2)
        acc[0, :, columns] = acc[0, :, columns] * shrink + jnp.dot(
            vt[:, rows], p, preferred_element_type=F32
        )
        m_ref[0, 0:1, columns] = m_new

    def two(i, carry):
        step(2 * i, 0)
        step(2 * i + 1, 1)
        return carry

    lax.fori_loop(0, steps // 2, two, 0)
    if ends:
        for source in range(GROUPS):
            part = acc[0, :, source * OWN : (source + 1) * OWN]
            out_ref[source] = (part[:VDIM] / part[VDIM : VDIM + 1]).T.astype(BF16)


def attention(queries, pieces, weight, state=(), ends=False, bq=512, bk=512):
    sizes = tuple(p.shape[0] for p in pieces)
    keys = sum(sizes)
    state_shapes = (PER, VDIM + 16, ROWS), (PER, 8, ROWS)
    state_specs = [pl.BlockSpec((1, *shape[1:]), lambda h: (h, 0, 0)) for shape in state_shapes]
    if ends:
        out_specs = pl.BlockSpec((GROUPS, OWN, VDIM), lambda h: (0, 0, h))
        out_shape = jax.ShapeDtypeStruct((GROUPS, OWN, PER * VDIM), BF16)
        kept = [pltpu.VMEM((1, *shape[1:]), F32) for shape in state_shapes]
    else:
        out_specs = state_specs
        out_shape = [jax.ShapeDtypeStruct(shape, F32) for shape in state_shapes]
        kept = []
    return pl.pallas_call(
        functools.partial(attention_kernel, sizes, bq, bk, not state, ends),
        grid=(PER,),
        in_specs=[pl.BlockSpec((GROUPS, 1, QK, OWN), lambda h: (0, h, 0, 0))]
        + [pl.BlockSpec((size, WIDE), lambda h: (0, 0)) for size in sizes]
        + [pl.BlockSpec((RANK, NOPE + VDIM), lambda h: (0, h))]
        + (state_specs if state else []),
        out_specs=out_specs,
        out_shape=out_shape,
        scratch_shapes=kept
        + [
            pltpu.VMEM((keys, 256), BF16),
            pltpu.VMEM((VDIM + 16, keys), BF16),
            pltpu.VMEM((2, bk, bq), F32),
            pltpu.VMEM((256, ROWS), BF16),
        ],
        cost_estimate=pl.CostEstimate(
            flops=2 * PER * keys * (RANK * 256 + ROWS * 768),
            bytes_accessed=keys * WIDE * 2 + 6 * 2**20,
            transcendentals=PER * ROWS * keys,
        ),
        compiler_params=pltpu.CompilerParams(
            dimension_semantics=("arbitrary",), vmem_limit_bytes=40 * 2**20
        ),
    )(queries, *pieces, weight, *state)


def gate_kernel(heads_ref, gate_ref, gain_ref, out_ref, gated):
    total = jnp.zeros((OWN, 1), F32)
    for group in range(GROUPS):
        columns = slice(group * PER * VDIM, (group + 1) * PER * VDIM)
        v = gate_ref[:, columns].astype(F32)
        part = heads_ref[group].astype(F32) * (v * jax.nn.sigmoid(v))
        gated[:, columns] = part
        total += jnp.sum(part * part, axis=-1, keepdims=True)
    scale = lax.rsqrt(total / (HEADS * VDIM) + EPS)
    for group in range(GROUPS):
        columns = slice(group * PER * VDIM, (group + 1) * PER * VDIM)
        out_ref[:, columns] = (gated[:, columns] * scale * gain_ref[:, columns]).astype(BF16)


def shifted(value, axis, by):
    length = lax.axis_size(axis)
    return lax.ppermute(value, axis, [(i, (i + by) % length) for i in range(length)])


def along(move, mesh_shape):
    zh_n, zl_n, y_n, x_n, core_n = mesh_shape
    pairs = []
    for column in range(zh_n * zl_n * y_n):
        group, first = column % (zl_n * y_n), column * x_n * core_n
        for source, target in move(group // core_n, group % core_n, x_n):
            pairs.append((first + source, first + target))
    return pairs


def shard_of_group(weight, mesh_shape):
    def one_way(by):
        return along(lambda x, c, n: [(x * 2 + c, (x + by) % n * 2 + c)], mesh_shape)

    def far(by):
        return along(lambda x, c, n: [((x + by) % n * 2 + c, (x + 2) % n * 2 + c)], mesh_shape)

    swap = along(lambda x, c, n: [(i * 2 + c, i * 2 + 1 - c) for i in range(n)], mesh_shape)
    group = lax.axis_index(("zl", "y"))
    mine = lax.axis_index(DP) == group
    half = weight.shape[0] // 2
    right = lax.ppermute(weight, EVERY, one_way(1))
    left = lax.ppermute(weight, EVERY, one_way(-1))
    after = yield
    right, left, after = lax.optimization_barrier((right, left, after))
    top = lax.ppermute(right[:half], EVERY, far(1))
    bottom = lax.ppermute(left[half:], EVERY, far(-1))
    after = yield after
    top, bottom, after = lax.optimization_barrier((top, bottom, after))
    held = jnp.where(mine, weight, right + left + jnp.concatenate([top, bottom]))
    other = lax.ppermute(held, EVERY, swap)
    yield jnp.where(lax.axis_index("core") == group % 2, held, other)


def per_device(mesh_shape, queries, latent, rope_key, latent_gain, kv_weight, gate, out_gain):
    position = lax.axis_index(SP) * OWN + jnp.arange(OWN, dtype=jnp.int32)
    half = ROPE // 2
    inverse = THETA ** (-jnp.arange(half, dtype=F32) / half)
    angles = position.astype(F32)[:, None] * inverse[None, :]
    cosine, sine = jnp.cos(angles), jnp.sin(angles)

    sent = call(latent_kernel, (OWN, WIDE), 10**6, 2**20)(
        latent, rope_key, latent_gain[None, :], cosine, sine
    )
    queries, kv_weight, sent = lax.optimization_barrier((queries, kv_weight, sent))
    head_queries = call(query_kernel, (GROUPS // 2, 2, PER, QK, OWN), 10**7, 3 * 2**20)(
        queries, cosine, sine
    )
    weight_steps = shard_of_group(kv_weight, mesh_shape)
    next(weight_steps)
    blocks, (ahead, behind) = [sent], (sent, sent)
    for step in range(3):
        ahead, behind = shifted(ahead, Z, 1), shifted(behind, Z, -1)
        blocks += [ahead, behind]
        if step == 0:
            head_queries, ahead, behind = lax.optimization_barrier((head_queries, ahead, behind))
    ahead, behind = weight_steps.send((ahead, behind))
    half = OWN // 2
    blocks += [shifted(ahead[:half], Z, 1), shifted(behind[half:], Z, -1)]
    column = jnp.concatenate(blocks)

    head_queries = lax.all_to_all(head_queries, "y", 0, 0, tiled=True)
    zl = lax.axis_index("zl")
    mine = jnp.where(zl == 0, head_queries[:, 0], head_queries[:, 1])
    other = jnp.where(zl == 0, head_queries[:, 1], head_queries[:, 0])
    other = shifted(other, "zl", 1)
    pair = jnp.where(zl == 0, mine, other), jnp.where(zl == 0, other, mine)
    head_queries = jnp.concatenate(pair)

    weight = weight_steps.send(column)
    state = attention(head_queries, [column], weight)
    ahead, behind = shifted(column, "y", 1), shifted(column, "y", -1)
    ahead, behind, state = lax.optimization_barrier((ahead, behind, state))
    far = [shifted(ahead[: ROWS // 2], "y", 1), shifted(behind[ROWS // 2 :], "y", -1)]
    state = attention(head_queries, [ahead, behind], weight, state)
    heads_out = attention(head_queries, far, weight, state, ends=True)
    heads_out = lax.all_to_all(heads_out, ("zl", "y"), 0, 0, tiled=True)
    return call(
        gate_kernel,
        (OWN, HEADS * VDIM),
        10**7,
        3 * 2**20,
        scratch_shapes=[pltpu.VMEM((OWN, HEADS * VDIM), F32)],
    )(heads_out, gate, out_gain[None, :])


def solution(mesh):
    x_n, z_n, y_n = mesh.shape["dp"] // 2, 8, mesh.shape["sp"] // 8
    mesh_shape = (z_n // 2, 2, y_n, x_n, 2)
    named = Mesh(mesh.devices.reshape(mesh_shape), EVERY)
    tokens = P(("x", "core", "zh", "zl", "y"), None)

    def body(*operands):
        return per_device(mesh_shape, *operands)

    return jax.shard_map(
        body,
        mesh=named,
        in_specs=(tokens, tokens, tokens, P(), P(None, DP), tokens, P()),
        out_specs=tokens,
        check_vma=False,
    )
```

time: 194 us -> 192 us (0.990); the launches traced: 193 us -> 188 us
  starting transfers between devices: 61.4 us -> 42.3 us
  waiting for transfers between devices: 46.7 us -> 60 us
  other arithmetic: 8.61 us -> 12.8 us
    ppermute x24 -> x13, starting transfers between devices: 47.3 us -> 30.9 us  [shifted(): lax.ppermute(value, axis, [(i, (i + by) % length) for i in range(length)])]
    ppermute x24 -> x13, waiting for transfers between devices: 46.7 us -> 59.9 us  [shifted(): lax.ppermute(value, axis, [(i, (i + by) % length) for i in range(length)])]
    select_n x2 -> x4, other arithmetic: 7.46 us -> 11.7 us  [the longest x1 6.52 us: shard_of_group(): jnp.where(mine, weight, right + left + jnp.concatenate([top, bottom]))]
    all_to_all x1, starting transfers between devices: 8.34 us -> 4.35 us  [per_device(): head_queries = lax.all_to_all(head_queries, 'y', 0, 0, tiled=True)]
    slice x11 -> x6, local copies, waits for them, and re-layouts: 5.29 us -> 4.07 us  [the longest x1 1.36 us: per_device(): behind[ROWS // 2:]]
    pallas_call x4 -> x6, Pallas kernels: 48.3 us -> 47.9 us  [the longest x3 39.4 us: attention(): pl.pallas_call(functools.partial(attention_kernel, sizes, bq, bk, not sta...]
  transfers between devices with their start and end apart: 30 -> 19, of which waited for: 10 -> 10; matrix products, arithmetic and copies ran while one was open for 8% -> 9% of each run, Pallas kernels for 3% -> 17%
where the time goes in v2:
time: 192 us; the launch traced here: 188 us
  waiting for transfers between devices  60 us (31%)
  Pallas kernels  47.9 us (25%)
  starting transfers between devices  42.3 us (22%)
  blocking collectives  18.2 us (9%)
  other arithmetic  12.8 us (7%)
  local copies, waits for them, and re-layouts  7.01 us (4%)
    ppermute x13, waiting for transfers between devices, shifted(): lax.ppermute(value, axis, [(i, (i + by) % length) for i in range(length)])  59.9 us
    pallas_call x3, Pallas kernels, attention(): pl.pallas_call(functools.partial(attention_kernel, sizes, bq, bk, not sta...  39.4 us
    ppermute x13, starting transfers between devices, shifted(): lax.ppermute(value, axis, [(i, (i + by) % length) for i in range(length)])  30.9 us
    all_to_all x1, blocking collectives, per_device(): heads_out = lax.all_to_all(heads_out, ('zl', 'y'), 0, 0, tiled=True)  18.2 us
    select_n x1, other arithmetic, shard_of_group(): jnp.where(mine, weight, right + left + jnp.concatenate([top, bottom]))  6.52 us
    all_to_all x1, starting transfers between devices, per_device(): head_queries = lax.all_to_all(head_queries, 'y', 0, 0, tiled=True)  4.35 us
  transfers between devices with their start and end apart: 19, of which 10 were waited for; matrix products, arithmetic and copies ran while one was open for 9% of the time, Pallas kernels for 17%

profile of v2, /device:TPU:8, one launch (start us, length us, event | category | flops | bytes accessed | tf_op | source)
XLA Modules:
  0.0 188.4 jit_solution(15873767230435439009)
XLA Ops:
  0.0 1.4 copy.10.key_ref
  1.5 1.0 multiply_sine_fusion
  2.4 2.0 %shard_map.73 = bf16[128,1152]{1,0:T(8,128)(2,1)} custom-call(bf16[128,1024]{1,0:T(8,128)(2,1)} %latent_ref.1, bf16[128,64]{1,0:T(8,128)(2,1)} %copy.10.key_ref, f32[1,1024]{1,0:T(1,128)} %bitcast.28, f32[128,32]{1,0:T(8,128)} %get-tuple-element.48.cos_ref, f32[128,32]{1,0:T(8,128)} %get-tuple-element.47.sin_ref), custom_call_target="tpu_custom_call" | custom-call | flops 1000000 | bytes 1048576 | tf_op jit(solution)/shard_map/pallas_call | solution.py:244
  4.4 2.2 %collective-permute-start.7 = (bf16[1024,1024]{1,0:T(8,128)(2,1)}, bf16[1024,1024]{1,0:T(8,128)(2,1)}, u32[]{:S(2)}, u32[]{:S(2)}) collective-permute-start(bf16[1024,1024]{1,0:T(8,128)(2,1)} %param.11), channel_id=1, source_target_pairs={{0,2},{9,11},{18,20},{27,29},{36,38},{45,47},{54,48},{63,57},{64,6... | collective-permute-start | bytes 6291464 | tf_op jit(solution)/shard_map/ppermute | solution.py:224
  6.6 2.0 %collective-permute-start.8 = (bf16[1024,1024]{1,0:T(8,128)(2,1)}, bf16[1024,1024]{1,0:T(8,128)(2,1)}, u32[]{:S(2)}, u32[]{:S(2)}) collective-permute-start(bf16[1024,1024]{1,0:T(8,128)(2,1)} %param.11), channel_id=1, source_target_pairs={{0,6},{9,15},{18,16},{27,25},{36,34},{45,43},{54,52},{63,61},{64,7... | collective-permute-start | bytes 6291464 | tf_op jit(solution)/shard_map/ppermute | solution.py:225
  8.5 1.9 %collective-permute-start = (bf16[128,1152]{1,0:T(8,128)(2,1)}, bf16[128,1152]{1,0:T(8,128)(2,1)}, u32[]{:S(2)}, u32[]{:S(2)}) collective-permute-start(bf16[128,1152]{1,0:T(8,128)(2,1)} %shard_map.73), channel_id=1, source_target_pairs={{0,32},{32,64},{64,96},{96,128},{128,160},{160,192},{192,224},{224... | collective-permute-start | bytes 884744 | tf_op jit(solution)/shard_map/ppermute | solution.py:200
  10.5 3.9 %collective-permute-start.1 = (bf16[128,1152]{1,0:T(8,128)(2,1)}, bf16[128,1152]{1,0:T(8,128)(2,1)S(1)}, u32[]{:S(2)}, u32[]{:S(2)}) collective-permute-start(bf16[128,1152]{1,0:T(8,128)(2,1)} %shard_map.73), channel_id=1, source_target_pairs={{0,224},{32,0},{64,32},{96,64},{128,96},{160,128},{192,160},{224,1... | collective-permute-start | bytes 884744 | tf_op jit(solution)/shard_map/ppermute | solution.py:200
  14.4 3.1 %shard_map.74 = bf16[4,2,4,192,128]{4,3,2,1,0:T(8,128)(2,1)} custom-call(bf16[128,6144]{1,0:T(8,128)(2,1)} %q_ref, f32[128,32]{1,0:T(8,128)} %get-tuple-element.48.cos_ref, f32[128,32]{1,0:T(8,128)} %get-tuple-element.47.sin_ref), custom_call_target="tpu_custom_call" | custom-call | flops 10000000 | bytes 3145728 | tf_op jit(solution)/shard_map/pallas_call | solution.py:248
  17.5 5.0 %collective-permute-done = bf16[128,1152]{1,0:T(8,128)(2,1)} collective-permute-done((bf16[128,1152]{1,0:T(8,128)(2,1)}, bf16[128,1152]{1,0:T(8,128)(2,1)}, u32[]{:S(2)}, u32[]{:S(2)}) %collective-permute-start) | collective-permute-done | bytes 294944 | tf_op jit(solution)/shard_map/ppermute | solution.py:200
  22.5 3.2 %collective-permute-start.4 = (bf16[128,1152]{1,0:T(8,128)(2,1)S(1)}, bf16[128,1152]{1,0:T(8,128)(2,1)S(1)}, u32[]{:S(2)}, u32[]{:S(2)}) collective-permute-start(bf16[128,1152]{1,0:T(8,128)(2,1)S(1)} %collective-permute-done.1), channel_id=1, source_target_pairs={{0,224},{32,0},{64,32},{96,64},{128,96},{160,128},{192,160},{224,1... | collective-permute-start | bytes 884744 | tf_op jit(solution)/shard_map/ppermute | solution.py:200
  25.8 4.4 %all-to-all-start = ((bf16[4,2,4,192,128]{4,3,2,1,0:T(8,128)(2,1)}), bf16[4,2,4,192,128]{4,3,2,1,0:T(8,128)(2,1)}, u32[]{:S(2)}, u32[]{:S(2)}) async-start(bf16[4,2,4,192,128]{4,3,2,1,0:T(8,128)(2,1)} %shard_map.74), calls=%async_computation | async-start | bytes 3145728 | tf_op jit(solution)/shard_map/all_to_all | solution.py:264
  30.2 1.0 constant_dynamic-update-slice_fusion.7
  31.2 1.8 collective-permute-done.3
  33.0 3.2 %collective-permute-start.6 = (bf16[128,1152]{1,0:T(8,128)(2,1)S(1)}, bf16[128,1152]{1,0:T(8,128)(2,1)S(1)}, u32[]{:S(2)}, u32[]{:S(2)}) collective-permute-start(bf16[128,1152]{1,0:T(8,128)(2,1)S(1)} %collective-permute-done.4), channel_id=1, source_target_pairs={{0,224},{32,0},{64,32},{96,64},{128,96},{160,128},{192,160},{224,1... | collective-permute-start | bytes 884744 | tf_op jit(solution)/shard_map/ppermute | solution.py:200
  36.3 6.0 %collective-permute-done.5 = bf16[128,1152]{1,0:T(8,128)(2,1)S(1)} collective-permute-done((bf16[128,1152]{1,0:T(8,128)(2,1)S(1)}, bf16[128,1152]{1,0:T(8,128)(2,1)S(1)}, u32[]{:S(2)}, u32[]{:S(2)}) %collective-permute-start.5) | collective-permute-done | bytes 294944 | tf_op jit(solution)/shard_map/ppermute | solution.py:200
  42.3 1.3 slice.30
  43.6 0.0 copy-start.2
  43.6 0.9 collective-permute-start.13
  44.5 1.3 slice.31
  45.8 0.7 collective-permute-start.14
  46.6 1.6 collective-permute-start.9
  48.3 1.8 collective-permute-start.10
  50.1 3.0 %collective-permute-done.9 = bf16[64,1152]{1,0:T(8,128)(2,1)S(1)} collective-permute-done((bf16[64,1152]{1,0:T(8,128)(2,1)S(1)}, bf16[64,1152]{1,0:T(8,128)(2,1)S(1)}, u32[]{:S(2)}, u32[]{:S(2)}) %collective-permute-start.9) | collective-permute-done | bytes 147488 | tf_op jit(solution)/shard_map/ppermute | solution.py:200
  53.1 0.5 collective-permute-done.10
  53.6 6.5 %fusion = bf16[1024,1024]{1,0:T(8,128)(2,1)} fusion(bf16[1024,1024]{1,0:T(8,128)(2,1)S(1)} %copy-done.2, bf16[512,1024]{1,0:T(8,128)(2,1)S(1)} %collective-permute-done.14, bf16[512,1024]{1,0:T(8,128)(2,1)S(1)} %collective-permute-done.13, bf16[1024,1024]{1,0:T(8,128)(2,1)} %collective-permute-done.7, bf16[1024,1024]{1,0:T(8,128)(2,1)} %collective-permute-done.8, ...), kind=kLoop, calls=%fused_computation.1 | loop fusion | flops 9437184 | bytes 10485761 | tf_op jit(solution)/shard_map/jit(_where)/select_n | solution.py:232
  60.1 1.3 collective-permute-start.15
  61.4 1.5 select_bitcast_fusion
  62.9 2.5 %collective-permute-start.2 = (bf16[4,4,192,128]{3,2,1,0:T(8,128)(2,1)S(1)}, bf16[4,4,192,128]{3,2,1,0:T(8,128)(2,1)}, u32[]{:S(2)}, u32[]{:S(2)}) collective-permute-start(bf16[4,4,192,128]{3,2,1,0:T(8,128)(2,1)S(1)} %select_bitcast_fusion), channel_id=1, source_target_pairs={{0,32},{32,0},{1,33},{33,1},{2,34},{34,2},{3,35},{35,3},{4,36},{36... | collective-permute-start | bytes 2359304 | tf_op jit(solution)/shard_map/ppermute | solution.py:200
  65.4 7.7 %collective-permute-start.11 = (bf16[1024,1152]{1,0:T(8,128)(2,1)}, bf16[1024,1152]{1,0:T(8,128)(2,1)S(1)}, u32[]{:S(2)}, u32[]{:S(2)}) collective-permute-start(bf16[1024,1152]{1,0:T(8,128)(2,1)} %copy-done), channel_id=1, source_target_pairs={{0,8},{8,16},{16,24},{24,0},{1,9},{9,17},{17,25},{25,1},{2,10},{10... | collective-permute-start | bytes 7077896 | tf_op jit(solution)/shard_map/ppermute | solution.py:200
  73.2 2.7 %collective-permute-start.12 = (bf16[1024,1152]{1,0:T(8,128)(2,1)}, bf16[1024,1152]{1,0:T(8,128)(2,1)}, u32[]{:S(2)}, u32[]{:S(2)}) collective-permute-start(bf16[1024,1152]{1,0:T(8,128)(2,1)} %copy-done), channel_id=1, source_target_pairs={{0,24},{8,0},{16,8},{24,16},{1,25},{9,1},{17,9},{25,17},{2,26},{10... | collective-permute-start | bytes 7077896 | tf_op jit(solution)/shard_map/ppermute | solution.py:200
  75.9 4.1 %collective-permute-done.2 = bf16[4,4,192,128]{3,2,1,0:T(8,128)(2,1)} collective-permute-done((bf16[4,4,192,128]{3,2,1,0:T(8,128)(2,1)S(1)}, bf16[4,4,192,128]{3,2,1,0:T(8,128)(2,1)}, u32[]{:S(2)}, u32[]{:S(2)}) %collective-permute-start.2) | collective-permute-done | bytes 786464 | tf_op jit(solution)/shard_map/ppermute | solution.py:200
  79.9 1.7 bitcast_select_fusion.1
  81.7 0.1 pad_maximum_fusion.q_ref
  81.8 2.0 %broadcast_select_fusion.refs_1_.refs_2_ = bf16[1024,1024]{1,0:T(8,128)(2,1)S(1)} fusion(bf16[1024,1024]{1,0:T(8,128)(2,1)} %fusion, bf16[1024,1024]{1,0:T(8,128)(2,1)} %collective-permute-done.15, pred[]{:T(512)S(6)} %eq.15), kind=kLoop, calls=%fused_computation.2 | loop fusion | flops 1048576 | bytes 6291457 | tf_op jit(solution)/shard_map/jit(_where)/select_n | solution.py:234
  83.8 0.3 copy-done.1
  84.1 9.6 %shard_map.75 = (f32[4,144,1024]{2,1,0:T(8,128)S(1)}, f32[4,8,1024]{2,1,0:T(8,128)S(1)}) custom-call(bf16[8,4,192,128]{3,2,1,0:T(8,128)(2,1)S(1)} %pad_maximum_fusion.q_ref, bf16[1024,1152]{1,0:T(8,128)(2,1)S(1)} %copy-done.1, bf16[1024,1024]{1,0:T(8,128)(2,1)S(1)} %broadcast_select_fusion.refs_1_.refs_2_), custom_call_target="tpu_custom_call" | custom-call | flops 8589934592 | bytes 8650752 | tf_op jit(solution)/shard_map/pallas_call | solution.py:157
  93.7 29.5 %collective-permute-done.11.refs_0_ = bf16[1024,1152]{1,0:T(8,128)(2,1)S(1)} collective-permute-done((bf16[1024,1152]{1,0:T(8,128)(2,1)}, bf16[1024,1152]{1,0:T(8,128)(2,1)S(1)}, u32[]{:S(2)}, u32[]{:S(2)}) %collective-permute-start.11) | collective-permute-done | bytes 2359328 | tf_op jit(solution)/shard_map/ppermute | solution.py:200
  123.2 4.1 %collective-permute-done.12.refs_1_ = bf16[1024,1152]{1,0:T(8,128)(2,1)} collective-permute-done((bf16[1024,1152]{1,0:T(8,128)(2,1)}, bf16[1024,1152]{1,0:T(8,128)(2,1)}, u32[]{:S(2)}, u32[]{:S(2)}) %collective-permute-start.12) | collective-permute-done | bytes 2359328 | tf_op jit(solution)/shard_map/ppermute | solution.py:200
  127.2 0.1 slice.32
  127.3 1.8 collective-permute-start.16
  129.1 1.4 slice.33
  130.5 0.4 collective-permute-start.17
  130.9 19.5 %shard_map.76 = (f32[4,144,1024]{2,1,0:T(8,128)S(1)}, f32[4,8,1024]{2,1,0:T(8,128)S(1)}) custom-call(bf16[8,4,192,128]{3,2,1,0:T(8,128)(2,1)S(1)} %pad_maximum_fusion.q_ref, bf16[1024,1152]{1,0:T(8,128)(2,1)S(1)} %collective-permute-done.11.refs_0_, bf16[1024,1152]{1,0:T(8,128)(2,1)} %collective-permute-done.12.refs_1_, ...), custom_call_target="tpu_custom_call" | custom-call | flops 17179869184 | bytes 11010048 | tf_op jit(solution)/shard_map/pallas_call | solution.py:157
  150.4 4.6 %collective-permute-done.16.refs_0_ = bf16[512,1152]{1,0:T(8,128)(2,1)S(1)} collective-permute-done((bf16[512,1152]{1,0:T(8,128)(2,1)S(1)}, bf16[512,1152]{1,0:T(8,128)(2,1)S(1)}, u32[]{:S(2)}, u32[]{:S(2)}) %collective-permute-start.16) | collective-permute-done | bytes 1179680 | tf_op jit(solution)/shard_map/ppermute | solution.py:200
  155.0 1.5 collective-permute-done.17.refs_1_
  156.5 10.3 %shard_map.77 = bf16[8,128,512]{2,1,0:T(8,128)(2,1)S(1)} custom-call(bf16[8,4,192,128]{3,2,1,0:T(8,128)(2,1)S(1)} %pad_maximum_fusion.q_ref, bf16[512,1152]{1,0:T(8,128)(2,1)S(1)} %collective-permute-done.16.refs_0_, bf16[512,1152]{1,0:T(8,128)(2,1)S(1)} %collective-permute-done.17.refs_1_, bf16[1024,1024]{1,0:T(8,128)(2,1)S(1)} %broadcast_select_fusion.refs_1_.refs_2_, ...), custom_call_target="tpu_custom_call" | custom-call | flops 8589934592 | bytes 8650752 | tf_op jit(solution)/shard_map/pallas_call | solution.py:157
  166.8 18.2 %all_to_all.10.heads_ref = bf16[8,128,512]{2,1,0:T(8,128)(2,1)} all-to-all(bf16[8,128,512]{2,1,0:T(8,128)(2,1)S(1)} %shard_map.77), channel_id=1, replica_groups=mesh['zh'=4,'zl'=2,'y'=4,'x'=4,'core'=2] {'zl','y'}, dimensions={0} | all-to-all | bytes 2097152 | tf_op jit(solution)/shard_map/all_to_all | solution.py:279
  185.0 3.4 %shard_map.78 = bf16[128,4096]{1,0:T(8,128)(2,1)} custom-call(bf16[8,128,512]{2,1,0:T(8,128)(2,1)} %all_to_all.10.heads_ref, bf16[128,4096]{1,0:T(8,128)(2,1)} %gate_ref.1, f32[1,4096]{1,0:T(1,128)} %bitcast.27), custom_call_target="tpu_custom_call" | custom-call | flops 10000000 | bytes 3145728 | tf_op jit(solution)/shard_map/pallas_call | solution.py:280
  (29 shorter events, 0.3 us)
Async XLA Ops:
  4.4 21.4 %copy-start.3 = (bf16[128,1152]{1,0:T(8,128)(2,1)S(1)}, bf16[128,1152]{1,0:T(8,128)(2,1)}, u32[]{:S(2)}) copy-start(bf16[128,1152]{1,0:T(8,128)(2,1)} %shard_map.73) | copy-start | bytes 884740
  4.4 37.9 %collective-permute-start.7 = (bf16[1024,1024]{1,0:T(8,128)(2,1)}, bf16[1024,1024]{1,0:T(8,128)(2,1)}, u32[]{:S(2)}, u32[]{:S(2)}) collective-permute-start(bf16[1024,1024]{1,0:T(8,128)(2,1)} %param.11), channel_id=1, source_target_pairs={{0,2},{9,11},{18,20},{27,29},{36,38},{45,47},{54,48},{63,57},{64,6... | collective-permute-start | bytes 6291464 | tf_op jit(solution)/shard_map/ppermute | solution.py:224
  6.6 35.8 %collective-permute-start.8 = (bf16[1024,1024]{1,0:T(8,128)(2,1)}, bf16[1024,1024]{1,0:T(8,128)(2,1)}, u32[]{:S(2)}, u32[]{:S(2)}) collective-permute-start(bf16[1024,1024]{1,0:T(8,128)(2,1)} %param.11), channel_id=1, source_target_pairs={{0,6},{9,15},{18,16},{27,25},{36,34},{45,43},{54,52},{63,61},{64,7... | collective-permute-start | bytes 6291464 | tf_op jit(solution)/shard_map/ppermute | solution.py:225
  8.5 14.0 %collective-permute-start = (bf16[128,1152]{1,0:T(8,128)(2,1)}, bf16[128,1152]{1,0:T(8,128)(2,1)}, u32[]{:S(2)}, u32[]{:S(2)}) collective-permute-start(bf16[128,1152]{1,0:T(8,128)(2,1)} %shard_map.73), channel_id=1, source_target_pairs={{0,32},{32,64},{64,96},{96,128},{128,160},{160,192},{192,224},{224... | collective-permute-start | bytes 884744 | tf_op jit(solution)/shard_map/ppermute | solution.py:200
  10.5 12.1 %collective-permute-start.1 = (bf16[128,1152]{1,0:T(8,128)(2,1)}, bf16[128,1152]{1,0:T(8,128)(2,1)S(1)}, u32[]{:S(2)}, u32[]{:S(2)}) collective-permute-start(bf16[128,1152]{1,0:T(8,128)(2,1)} %shard_map.73), channel_id=1, source_target_pairs={{0,224},{32,0},{64,32},{96,64},{128,96},{160,128},{192,160},{224,1... | collective-permute-start | bytes 884744 | tf_op jit(solution)/shard_map/ppermute | solution.py:200
  22.5 10.4 %collective-permute-start.3 = (bf16[128,1152]{1,0:T(8,128)(2,1)}, bf16[128,1152]{1,0:T(8,128)(2,1)S(1)}, u32[]{:S(2)}, u32[]{:S(2)}) collective-permute-start(bf16[128,1152]{1,0:T(8,128)(2,1)} %collective-permute-done), channel_id=1, source_target_pairs={{0,32},{32,64},{64,96},{96,128},{128,160},{160,192},{192,224},{224... | collective-permute-start | bytes 884744 | tf_op jit(solution)/shard_map/ppermute | solution.py:200
  22.5 10.4 %collective-permute-start.4 = (bf16[128,1152]{1,0:T(8,128)(2,1)S(1)}, bf16[128,1152]{1,0:T(8,128)(2,1)S(1)}, u32[]{:S(2)}, u32[]{:S(2)}) collective-permute-start(bf16[128,1152]{1,0:T(8,128)(2,1)S(1)} %collective-permute-done.1), channel_id=1, source_target_pairs={{0,224},{32,0},{64,32},{96,64},{128,96},{160,128},{192,160},{224,1... | collective-permute-start | bytes 884744 | tf_op jit(solution)/shard_map/ppermute | solution.py:200
  25.8 35.6 %all-to-all-start = ((bf16[4,2,4,192,128]{4,3,2,1,0:T(8,128)(2,1)}), bf16[4,2,4,192,128]{4,3,2,1,0:T(8,128)(2,1)}, u32[]{:S(2)}, u32[]{:S(2)}) async-start(bf16[4,2,4,192,128]{4,3,2,1,0:T(8,128)(2,1)} %shard_map.74), calls=%async_computation | async-start | bytes 3145728 | tf_op jit(solution)/shard_map/all_to_all | solution.py:264
  33.0 9.3 %collective-permute-start.5 = (bf16[128,1152]{1,0:T(8,128)(2,1)S(1)}, bf16[128,1152]{1,0:T(8,128)(2,1)S(1)}, u32[]{:S(2)}, u32[]{:S(2)}) collective-permute-start(bf16[128,1152]{1,0:T(8,128)(2,1)S(1)} %collective-permute-done.3), channel_id=1, source_target_pairs={{0,32},{32,64},{64,96},{96,128},{128,160},{160,192},{192,224},{224... | collective-permute-start | bytes 884744 | tf_op jit(solution)/shard_map/ppermute | solution.py:200
  33.0 9.3 %collective-permute-start.6 = (bf16[128,1152]{1,0:T(8,128)(2,1)S(1)}, bf16[128,1152]{1,0:T(8,128)(2,1)S(1)}, u32[]{:S(2)}, u32[]{:S(2)}) collective-permute-start(bf16[128,1152]{1,0:T(8,128)(2,1)S(1)} %collective-permute-done.4), channel_id=1, source_target_pairs={{0,224},{32,0},{64,32},{96,64},{128,96},{160,128},{192,160},{224,1... | collective-permute-start | bytes 884744 | tf_op jit(solution)/shard_map/ppermute | solution.py:200
  43.6 10.0 %copy-start.2 = (bf16[1024,1024]{1,0:T(8,128)(2,1)S(1)}, bf16[1024,1024]{1,0:T(8,128)(2,1)}, u32[]{:S(2)}) copy-start(bf16[1024,1024]{1,0:T(8,128)(2,1)} %param.11) | copy-start | bytes 6291460
  43.6 9.9 %collective-permute-start.13 = (bf16[512,1024]{1,0:T(8,128)(2,1)S(1)}, bf16[512,1024]{1,0:T(8,128)(2,1)S(1)}, u32[]{:S(2)}, u32[]{:S(2)}) collective-permute-start(bf16[512,1024]{1,0:T(8,128)(2,1)S(1)} %slice.30), channel_id=1, source_target_pairs={{2,4},{11,13},{20,22},{29,31},{38,32},{47,41},{48,50},{57,59},{66,... | collective-permute-start | bytes 3145736 | tf_op jit(solution)/shard_map/ppermute | solution.py:228
  45.8 7.8 %collective-permute-start.14 = (bf16[512,1024]{1,0:T(8,128)(2,1)S(1)}, bf16[512,1024]{1,0:T(8,128)(2,1)S(1)}, u32[]{:S(2)}, u32[]{:S(2)}) collective-permute-start(bf16[512,1024]{1,0:T(8,128)(2,1)S(1)} %slice.31), channel_id=1, source_target_pairs={{6,4},{15,13},{16,22},{25,31},{34,32},{43,41},{52,50},{61,59},{70,... | collective-permute-start | bytes 3145736 | tf_op jit(solution)/shard_map/ppermute | solution.py:229
  46.6 6.4 %collective-permute-start.9 = (bf16[64,1152]{1,0:T(8,128)(2,1)S(1)}, bf16[64,1152]{1,0:T(8,128)(2,1)S(1)}, u32[]{:S(2)}, u32[]{:S(2)}) collective-permute-start(bf16[64,1152]{1,0:T(8,128)(2,1)S(1)} %slice.28), channel_id=1, source_target_pairs={{0,32},{32,64},{64,96},{96,128},{128,160},{160,192},{192,224},{224... | collective-permute-start | bytes 442376 | tf_op jit(solution)/shard_map/ppermute | solution.py:200
  48.3 5.2 %collective-permute-start.10 = (bf16[64,1152]{1,0:T(8,128)(2,1)S(1)}, bf16[64,1152]{1,0:T(8,128)(2,1)S(1)}, u32[]{:S(2)}, u32[]{:S(2)}) collective-permute-start(bf16[64,1152]{1,0:T(8,128)(2,1)S(1)} %slice.29), channel_id=1, source_target_pairs={{0,224},{32,0},{64,32},{96,64},{128,96},{160,128},{192,160},{224,1... | collective-permute-start | bytes 442376 | tf_op jit(solution)/shard_map/ppermute | solution.py:200
  53.6 9.3 %copy-start = (bf16[1024,1152]{1,0:T(8,128)(2,1)}, bf16[1024,1152]{1,0:T(8,128)(2,1)S(1)}, u32[]{:S(2)}) copy-start(bf16[1024,1152]{1,0:T(8,128)(2,1)S(1)} %constant_dynamic-update-slice_fusion.refs_0_) | copy-start | bytes 7077892
  60.1 21.7 %collective-permute-start.15 = (bf16[1024,1024]{1,0:T(8,128)(2,1)}, bf16[1024,1024]{1,0:T(8,128)(2,1)}, u32[]{:S(2)}, u32[]{:S(2)}) collective-permute-start(bf16[1024,1024]{1,0:T(8,128)(2,1)} %fusion), channel_id=1, source_target_pairs={{0,1},{2,3},{4,5},{6,7},{9,8},{11,10},{13,12},{15,14},{16,17},{18,... | collective-permute-start | bytes 6291464 | tf_op jit(solution)/shard_map/ppermute | solution.py:233
  62.9 17.0 %collective-permute-start.2 = (bf16[4,4,192,128]{3,2,1,0:T(8,128)(2,1)S(1)}, bf16[4,4,192,128]{3,2,1,0:T(8,128)(2,1)}, u32[]{:S(2)}, u32[]{:S(2)}) collective-permute-start(bf16[4,4,192,128]{3,2,1,0:T(8,128)(2,1)S(1)} %select_bitcast_fusion), channel_id=1, source_target_pairs={{0,32},{32,0},{1,33},{33,1},{2,34},{34,2},{3,35},{35,3},{4,36},{36... | collective-permute-start | bytes 2359304 | tf_op jit(solution)/shard_map/ppermute | solution.py:200
  65.4 57.7 %collective-permute-start.11 = (bf16[1024,1152]{1,0:T(8,128)(2,1)}, bf16[1024,1152]{1,0:T(8,128)(2,1)S(1)}, u32[]{:S(2)}, u32[]{:S(2)}) collective-permute-start(bf16[1024,1152]{1,0:T(8,128)(2,1)} %copy-done), channel_id=1, source_target_pairs={{0,8},{8,16},{16,24},{24,0},{1,9},{9,17},{17,25},{25,1},{2,10},{10... | collective-permute-start | bytes 7077896 | tf_op jit(solution)/shard_map/ppermute | solution.py:200
  73.2 54.1 %collective-permute-start.12 = (bf16[1024,1152]{1,0:T(8,128)(2,1)}, bf16[1024,1152]{1,0:T(8,128)(2,1)}, u32[]{:S(2)}, u32[]{:S(2)}) collective-permute-start(bf16[1024,1152]{1,0:T(8,128)(2,1)} %copy-done), channel_id=1, source_target_pairs={{0,24},{8,0},{16,8},{24,16},{1,25},{9,1},{17,9},{25,17},{2,26},{10... | collective-permute-start | bytes 7077896 | tf_op jit(solution)/shard_map/ppermute | solution.py:200
  81.8 2.3 %copy-start.1 = (bf16[1024,1152]{1,0:T(8,128)(2,1)S(1)}, bf16[1024,1152]{1,0:T(8,128)(2,1)}, u32[]{:S(2)}) copy-start(bf16[1024,1152]{1,0:T(8,128)(2,1)} %copy-done) | copy-start | bytes 7077892
  127.3 27.7 %collective-permute-start.16 = (bf16[512,1152]{1,0:T(8,128)(2,1)S(1)}, bf16[512,1152]{1,0:T(8,128)(2,1)S(1)}, u32[]{:S(2)}, u32[]{:S(2)}) collective-permute-start(bf16[512,1152]{1,0:T(8,128)(2,1)S(1)} %slice.32), channel_id=1, source_target_pairs={{0,8},{8,16},{16,24},{24,0},{1,9},{9,17},{17,25},{25,1},{2,10},{10... | collective-permute-start | bytes 3538952 | tf_op jit(solution)/shard_map/ppermute | solution.py:200
  130.5 26.0 %collective-permute-start.17 = (bf16[512,1152]{1,0:T(8,128)(2,1)S(1)}, bf16[512,1152]{1,0:T(8,128)(2,1)S(1)}, u32[]{:S(2)}, u32[]{:S(2)}) collective-permute-start(bf16[512,1152]{1,0:T(8,128)(2,1)S(1)} %slice.33), channel_id=1, source_target_pairs={{0,24},{8,0},{16,8},{24,16},{1,25},{9,1},{17,9},{25,17},{2,26},{10... | collective-permute-start | bytes 3538952 | tf_op jit(solution)/shard_map/ppermute | solution.py:200

commit v3 on v2

--- a/solution.py
+++ b/solution.py
@@ -20,7 +20,7 @@
 PER = HEADS // GROUPS
 OWN = 128
 ROWS = GROUPS * OWN
-WIDE = RANK + 2 * ROPE
+BLOCK = OWN + OWN * ROPE // RANK
 
 EPS = 1e-06
 THETA = 10000.0
@@ -49,12 +49,14 @@
 def latent_kernel(latent_ref, key_ref, gain_ref, cos_ref, sin_ref, sent_ref):
     wide = latent_ref[...].astype(F32)
     mean = jnp.mean(wide * wide, axis=-1, keepdims=True)
-    sent_ref[:, :RANK] = (wide * lax.rsqrt(mean + EPS) * gain_ref[...]).astype(BF16)
-    u1, u2 = key_ref[:, : ROPE // 2].astype(F32), key_ref[:, ROPE // 2 :].astype(F32)
+    sent_ref[:OWN, :] = (wide * lax.rsqrt(mean + EPS) * gain_ref[...]).astype(BF16)
+    key = key_ref[...].astype(F32).T
+    u1, u2 = key[:, : ROPE // 2], key[:, ROPE // 2 :]
     cosine, sine = cos_ref[...], sin_ref[...]
-    turned = [u1 * cosine - u2 * sine, u2 * cosine + u1 * sine]
-    turned.append(jnp.zeros((OWN, ROPE), F32))
-    sent_ref[:, RANK:] = jnp.concatenate(turned, axis=1).astype(BF16)
+    turned = jnp.concatenate([u1 * cosine - u2 * sine, u2 * cosine + u1 * sine], axis=1)
+    pairs = jnp.concatenate([turned[: OWN // 2], turned[OWN // 2 :]], axis=1)
+    packed = jnp.concatenate([pairs[i : i + 8] for i in range(0, OWN // 2, 8)], axis=1)
+    sent_ref[OWN:, :] = packed.astype(BF16)
 
 
 def query_kernel(q_ref, cos_ref, sin_ref, sent_ref):
@@ -74,6 +76,18 @@
             sent_ref[*to, NOPE:] = turned.astype(BF16)
 
 
+def joined_kernel(*refs):
+    start = 0
+    for ref in refs[:-1]:
+        refs[-1][start : start + ref.shape[0], :] = ref[...]
+        start += ref.shape[0]
+
+
+def joined(pieces):
+    rows = sum(p.shape[0] for p in pieces)
+    return call(joined_kernel, (rows, RANK), 10**6, 4 * rows * RANK)(*pieces)
+
+
 def attention_kernel(sizes, bq, bk, begins, ends, q_ref, *refs):
     pieces, refs = refs[: len(sizes)], refs[len(sizes) :]
     w_ref, refs = refs[0], refs[1:]
@@ -85,16 +99,23 @@
 
     row = lax.broadcasted_iota(jnp.int32, (16, keys), 0)
     vt[VDIM:, :] = jnp.where(row == 0, 1.0, 0.0).astype(BF16)
+    lane = lax.broadcasted_iota(jnp.int32, (OWN, 128), 1)
     start = 0
     for size, piece in zip(sizes, pieces):
-        step = min(size, 512)
-        for at in range(0, size, step):
-            kv = jnp.dot(piece[at : at + step, :RANK], w_ref[...], preferred_element_type=F32)
-            rows = slice(start, start + step)
-            kext[rows, :NOPE] = kv[:, :NOPE].astype(BF16)
-            kext[rows, NOPE:] = piece[at : at + step, RANK:]
-            vt[:VDIM, rows] = kv[:, NOPE:].T.astype(BF16)
-            start += step
+        for at in range(0, size, 4 * BLOCK):
+            step = min(4 * BLOCK, size - at)
+            kv = jnp.dot(piece[at : at + step, :], w_ref[...], preferred_element_type=F32)
+            for block in range(0, step, BLOCK):
+                rows = slice(start, start + OWN)
+                kext[rows, :NOPE] = kv[block : block + OWN, :NOPE].astype(BF16)
+                vt[:VDIM, rows] = kv[block : block + OWN, NOPE:].T.astype(BF16)
+                packed = piece[at + block + OWN : at + block + BLOCK, :].astype(F32)
+                pairs = jnp.concatenate(
+                    [packed[:, i : i + 128] for i in range(0, RANK, 128)], axis=0
+                )
+                both = jnp.concatenate([pairs, pltpu.roll(pairs, ROPE, 1)], axis=0)
+                kext[rows, NOPE:] = jnp.where(lane < ROPE, both, 0.0).astype(BF16)
+                start += OWN
     for source in range(GROUPS):
         q[:QK, source * OWN : (source + 1) * OWN] = q_ref[source, 0]
     q[QK:, :] = jnp.zeros((256 - QK, ROWS), BF16)
@@ -141,9 +162,9 @@
             out_ref[source] = (part[:VDIM] / part[VDIM : VDIM + 1]).T.astype(BF16)
 
 
-def attention(queries, pieces, weight, state=(), ends=False, bq=512, bk=512):
+def attention(queries, pieces, weight, state=(), ends=False, bq=512, bk=1024):
     sizes = tuple(p.shape[0] for p in pieces)
-    keys = sum(sizes)
+    keys = sum(sizes) // BLOCK * OWN
     state_shapes = (PER, VDIM + 16, ROWS), (PER, 8, ROWS)
     state_specs = [pl.BlockSpec((1, *shape[1:]), lambda h: (h, 0, 0)) for shape in state_shapes]
     if ends:
@@ -158,7 +179,7 @@
         functools.partial(attention_kernel, sizes, bq, bk, not state, ends),
         grid=(PER,),
         in_specs=[pl.BlockSpec((GROUPS, 1, QK, OWN), lambda h: (0, h, 0, 0))]
-        + [pl.BlockSpec((size, WIDE), lambda h: (0, 0)) for size in sizes]
+        + [pl.BlockSpec((size, RANK), lambda h: (0, 0)) for size in sizes]
         + [pl.BlockSpec((RANK, NOPE + VDIM), lambda h: (0, h))]
         + (state_specs if state else []),
         out_specs=out_specs,
@@ -172,7 +193,7 @@
         ],
         cost_estimate=pl.CostEstimate(
             flops=2 * PER * keys * (RANK * 256 + ROWS * 768),
-            bytes_accessed=keys * WIDE * 2 + 6 * 2**20,
+            bytes_accessed=sum(sizes) * RANK * 2 + 6 * 2**20,
             transcendentals=PER * ROWS * keys,
         ),
         compiler_params=pltpu.CompilerParams(
@@ -210,6 +231,39 @@
     return pairs
 
 
+def pick_kernel(role_ref, own, right, left, top, bottom, out_ref, sem):
+    half = out_ref.shape[0] // 2
+    for role, source in ((0, own), (1, right), (3, left)):
+
+        @pl.when(role_ref[0] == role)
+        def _(source=source):
+            copy = pltpu.make_async_copy(source, out_ref, sem.at[0])
+            copy.start()
+            copy.wait()
+
+    @pl.when(role_ref[0] == 2)
+    def _():
+        first = pltpu.make_async_copy(top, out_ref.at[:half], sem.at[0])
+        second = pltpu.make_async_copy(bottom, out_ref.at[half:], sem.at[1])
+        first.start()
+        second.start()
+        first.wait()
+        second.wait()
+
+
+def picked(role, *sources):
+    return call(
+        pick_kernel,
+        sources[0].shape,
+        10**6,
+        2 * sources[0].size,
+        in_specs=[pl.BlockSpec(memory_space=pltpu.SMEM)]
+        + [pl.BlockSpec(memory_space=pl.ANY)] * len(sources),
+        out_specs=pl.BlockSpec(memory_space=pltpu.VMEM),
+        scratch_shapes=[pltpu.SemaphoreType.DMA((2,))],
+    )(role[None], *sources)
+
+
 def shard_of_group(weight, mesh_shape):
     def one_way(by):
         return along(lambda x, c, n: [(x * 2 + c, (x + by) % n * 2 + c)], mesh_shape)
@@ -219,17 +273,17 @@
 
     swap = along(lambda x, c, n: [(i * 2 + c, i * 2 + 1 - c) for i in range(n)], mesh_shape)
     group = lax.axis_index(("zl", "y"))
-    mine = lax.axis_index(DP) == group
     half = weight.shape[0] // 2
     right = lax.ppermute(weight, EVERY, one_way(1))
     left = lax.ppermute(weight, EVERY, one_way(-1))
-    after = yield
-    right, left, after = lax.optimization_barrier((right, left, after))
+    right, left = lax.optimization_barrier((right, left))
     top = lax.ppermute(right[:half], EVERY, far(1))
     bottom = lax.ppermute(left[half:], EVERY, far(-1))
-    after = yield after
+    after = yield
     top, bottom, after = lax.optimization_barrier((top, bottom, after))
-    held = jnp.where(mine, weight, right + left + jnp.concatenate([top, bottom]))
+    step_from = jnp.where(lax.axis_index("core") == group % 2, lax.axis_index("x") - group // 2, 0)
+    role = lax.rem(step_from + mesh_shape[3], mesh_shape[3])
+    held = picked(role, weight, right, left, top, bottom)
     other = lax.ppermute(held, EVERY, swap)
     yield jnp.where(lax.axis_index("core") == group % 2, held, other)
 
@@ -241,8 +295,8 @@
     angles = position.astype(F32)[:, None] * inverse[None, :]
     cosine, sine = jnp.cos(angles), jnp.sin(angles)
 
-    sent = call(latent_kernel, (OWN, WIDE), 10**6, 2**20)(
-        latent, rope_key, latent_gain[None, :], cosine, sine
+    sent = call(latent_kernel, (BLOCK, RANK), 10**6, 2**20)(
+        latent, rope_key.T, latent_gain[None, :], cosine, sine
     )
     queries, kv_weight, sent = lax.optimization_barrier((queries, kv_weight, sent))
     head_queries = call(query_kernel, (GROUPS // 2, 2, PER, QK, OWN), 10**7, 3 * 2**20)(
@@ -250,18 +304,15 @@
     )
     weight_steps = shard_of_group(kv_weight, mesh_shape)
     next(weight_steps)
+    head_queries = lax.all_to_all(head_queries, "y", 0, 0, tiled=True)
     blocks, (ahead, behind) = [sent], (sent, sent)
-    for step in range(3):
+    for _ in range(3):
         ahead, behind = shifted(ahead, Z, 1), shifted(behind, Z, -1)
         blocks += [ahead, behind]
-        if step == 0:
-            head_queries, ahead, behind = lax.optimization_barrier((head_queries, ahead, behind))
-    ahead, behind = weight_steps.send((ahead, behind))
-    half = OWN // 2
+    half = BLOCK // 2 + 4
     blocks += [shifted(ahead[:half], Z, 1), shifted(behind[half:], Z, -1)]
-    column = jnp.concatenate(blocks)
-
-    head_queries = lax.all_to_all(head_queries, "y", 0, 0, tiled=True)
+    first, second = joined(blocks[:4]), joined(blocks[4:])
+
     zl = lax.axis_index("zl")
     mine = jnp.where(zl == 0, head_queries[:, 0], head_queries[:, 1])
     other = jnp.where(zl == 0, head_queries[:, 1], head_queries[:, 0])
@@ -269,13 +320,13 @@
     pair = jnp.where(zl == 0, mine, other), jnp.where(zl == 0, other, mine)
     head_queries = jnp.concatenate(pair)
 
-    weight = weight_steps.send(column)
-    state = attention(head_queries, [column], weight)
-    ahead, behind = shifted(column, "y", 1), shifted(column, "y", -1)
-    ahead, behind, state = lax.optimization_barrier((ahead, behind, state))
-    far = [shifted(ahead[: ROWS // 2], "y", 1), shifted(behind[ROWS // 2 :], "y", -1)]
-    state = attention(head_queries, [ahead, behind], weight, state)
-    heads_out = attention(head_queries, far, weight, state, ends=True)
+    weight = weight_steps.send(second)
+    beside0 = [shifted(first, "y", 1), shifted(first, "y", -1)]
+    beside1 = [shifted(second, "y", 1), shifted(second, "y", -1)]
+    opposite = [shifted(beside0[0], "y", 1), shifted(beside1[1], "y", -1)]
+    state = attention(head_queries, [first, second], weight)
+    state = attention(head_queries, beside0 + beside1, weight, state)
+    heads_out = attention(head_queries, opposite, weight, state, ends=True)
     heads_out = lax.all_to_all(heads_out, ("zl", "y"), 0, 0, tiled=True)
     return call(
         gate_kernel,

time: 192 us -> 203 us (1.057)
  the two profiles are of different devices: /device:TPU:8 before, /device:TPU:70 now
where the time goes in v3:
time: 203 us
  waiting for transfers between devices  84.8 us (42%)
  Pallas kernels  54.6 us (27%)
  starting transfers between devices  33.6 us (17%)
  blocking collectives  20.7 us (10%)
  other arithmetic  4.45 us (2%)
  local copies, waits for them, and re-layouts  4.32 us (2%)
    ppermute x15, waiting for transfers between devices, shifted(): lax.ppermute(value, axis, [(i, (i + by) % length) for i in range(length)])  56.7 us
    pallas_call x3, Pallas kernels, attention(): pl.pallas_call(functools.partial(attention_kernel, sizes, bq, bk, not sta...  38.4 us
    ppermute x1, waiting for transfers between devices, shard_of_group(): left = lax.ppermute(weight, EVERY, one_way(-1))  28 us
    ppermute x15, starting transfers between devices, shifted(): lax.ppermute(value, axis, [(i, (i + by) % length) for i in range(length)])  21.4 us
    all_to_all x1, blocking collectives, per_device(): heads_out = lax.all_to_all(heads_out, ('zl', 'y'), 0, 0, tiled=True)  20.7 us
    pallas_call x2, Pallas kernels, joined(): return call(joined_kernel, (rows, RANK), 10 ** 6, 4 * rows * RANK)(*pieces)  4.6 us
    all_to_all x1, starting transfers between devices, per_device(): head_queries = lax.all_to_all(head_queries, 'y', 0, 0, tiled=True)  4.35 us
  transfers between devices with their start and end apart: 21, of which 9 were waited for; matrix products, arithmetic and copies ran while one was open for 2% of the time, Pallas kernels for 19%

profile of v3, /device:TPU:70, one launch (start us, length us, event | category | flops | bytes accessed | tf_op | source)
XLA Modules:
  0.0 202.5 jit_solution(3270820176165059474)
XLA Ops:
  0.0 0.9 multiply_sine_fusion
  1.0 2.0 shard_map.73.refs_0_
  3.0 0.9 collective-permute-start.13
  3.9 1.3 collective-permute-start.14
  5.2 28.0 %collective-permute-done.14.left = bf16[1024,1024]{1,0:T(8,128)(2,1)S(1)} collective-permute-done((bf16[1024,1024]{1,0:T(8,128)(2,1)}, bf16[1024,1024]{1,0:T(8,128)(2,1)S(1)}, u32[]{:S(2)}, u32[]{:S(2)}) %collective-permute-start.14) | collective-permute-done | bytes 2097184 | tf_op jit(solution)/shard_map/ppermute | solution.py:278
  33.2 0.1 slice.24
  33.3 0.7 collective-permute-start.15
  34.1 0.1 slice.25
  34.1 0.4 copy-done.4
  34.6 2.3 %collective-permute-start.16 = (bf16[512,1024]{1,0:T(8,128)(2,1)S(1)}, bf16[512,1024]{1,0:T(8,128)(2,1)}, u32[]{:S(2)}, u32[]{:S(2)}) collective-permute-start(bf16[512,1024]{1,0:T(8,128)(2,1)S(1)} %slice.25), channel_id=1, source_target_pairs={{6,4},{15,13},{16,22},{25,31},{34,32},{43,41},{52,50},{61,59},{70,... | collective-permute-start | bytes 3145736 | tf_op jit(solution)/shard_map/ppermute | solution.py:281
  36.8 0.0 collective-permute-start.1
  36.8 2.0 collective-permute-start.2
  38.9 4.6 %collective-permute-done.1.refs_1_ = bf16[136,1024]{1,0:T(8,128)(2,1)} collective-permute-done((bf16[136,1024]{1,0:T(8,128)(2,1)S(1)}, bf16[136,1024]{1,0:T(8,128)(2,1)}, u32[]{:S(2)}, u32[]{:S(2)}) %collective-permute-start.1) | collective-permute-done | bytes 278560 | tf_op jit(solution)/shard_map/ppermute | solution.py:221
  43.5 2.5 %collective-permute-start.3 = (bf16[136,1024]{1,0:T(8,128)(2,1)}, bf16[136,1024]{1,0:T(8,128)(2,1)}, u32[]{:S(2)}, u32[]{:S(2)}) collective-permute-start(bf16[136,1024]{1,0:T(8,128)(2,1)} %collective-permute-done.1.refs_1_), channel_id=1, source_target_pairs={{0,32},{32,64},{64,96},{96,128},{128,160},{160,192},{192,224},{224... | collective-permute-start | bytes 835592 | tf_op jit(solution)/shard_map/ppermute | solution.py:221
  45.9 0.6 collective-permute-done.2.refs_2_
  46.5 3.2 %shard_map.74 = bf16[4,2,4,192,128]{4,3,2,1,0:T(8,128)(2,1)} custom-call(bf16[128,6144]{1,0:T(8,128)(2,1)} %q_ref, f32[128,32]{1,0:T(8,128)} %get-tuple-element.30.cos_ref, f32[128,32]{1,0:T(8,128)} %get-tuple-element.29.sin_ref), custom_call_target="tpu_custom_call" | custom-call | flops 10000000 | bytes 3145728 | tf_op jit(solution)/shard_map/pallas_call | solution.py:302
  49.7 4.4 %all-to-all-start = ((bf16[4,2,4,192,128]{4,3,2,1,0:T(8,128)(2,1)}), bf16[4,2,4,192,128]{4,3,2,1,0:T(8,128)(2,1)}, u32[]{:S(2)}, u32[]{:S(2)}) async-start(bf16[4,2,4,192,128]{4,3,2,1,0:T(8,128)(2,1)} %shard_map.74), calls=%async_computation | async-start | bytes 3145728 | tf_op jit(solution)/shard_map/all_to_all | solution.py:307
  54.1 3.3 %collective-permute-start.7 = (bf16[136,1024]{1,0:T(8,128)(2,1)}, bf16[136,1024]{1,0:T(8,128)(2,1)S(1)}, u32[]{:S(2)}, u32[]{:S(2)}) collective-permute-start(bf16[136,1024]{1,0:T(8,128)(2,1)} %collective-permute-done.3.refs_3_), channel_id=1, source_target_pairs={{0,32},{32,64},{64,96},{96,128},{128,160},{160,192},{192,224},{224... | collective-permute-start | bytes 835592 | tf_op jit(solution)/shard_map/ppermute | solution.py:221
  57.4 5.8 %collective-permute-done.7.refs_1_ = bf16[136,1024]{1,0:T(8,128)(2,1)S(1)} collective-permute-done((bf16[136,1024]{1,0:T(8,128)(2,1)}, bf16[136,1024]{1,0:T(8,128)(2,1)S(1)}, u32[]{:S(2)}, u32[]{:S(2)}) %collective-permute-start.7) | collective-permute-done | bytes 278560 | tf_op jit(solution)/shard_map/ppermute | solution.py:221
  63.2 0.7 slice.28
  63.9 3.2 %collective-permute-start.9 = (bf16[72,1024]{1,0:T(8,128)(2,1)}, bf16[72,1024]{1,0:T(8,128)(2,1)}, u32[]{:S(2)}, u32[]{:S(2)}) collective-permute-start(bf16[72,1024]{1,0:T(8,128)(2,1)} %slice.28), channel_id=1, source_target_pairs={{0,32},{32,64},{64,96},{96,128},{128,160},{160,192},{192,224},{224... | collective-permute-start | bytes 442376 | tf_op jit(solution)/shard_map/ppermute | solution.py:221
  67.1 0.7 copy-done.8
  67.8 0.7 slice.29
  68.4 6.7 %collective-permute-done.10.refs_4_ = bf16[64,1024]{1,0:T(8,128)(2,1)S(1)} collective-permute-done((bf16[64,1024]{1,0:T(8,128)(2,1)}, bf16[64,1024]{1,0:T(8,128)(2,1)S(1)}, u32[]{:S(2)}, u32[]{:S(2)}) %collective-permute-start.10) | collective-permute-done | bytes 131104 | tf_op jit(solution)/shard_map/ppermute | solution.py:221
  75.2 0.7 copy-done.9
  75.9 2.3 %shard_map.76.refs_1_ = bf16[544,1024]{1,0:T(8,128)(2,1)} custom-call(bf16[136,1024]{1,0:T(8,128)(2,1)} %collective-permute-done.6.refs_0_, bf16[136,1024]{1,0:T(8,128)(2,1)} %copy-done.7, bf16[136,1024]{1,0:T(8,128)(2,1)} %copy-done.8, bf16[72,1024]{1,0:T(8,128)(2,1)} %collective-permute-done.9.refs_3_, bf16[64,1024]{1,0:T(8,128)(2,1)} %copy-done.9), custom_call_target="tpu_custom_call" | custom-call | flops 1000000 | bytes 2228224 | tf_op jit(solution)/shard_map/pallas_call | solution.py:88
  78.2 1.0 copy-done.6
  79.1 3.0 %shard_map.77 = bf16[1024,1024]{1,0:T(8,128)(2,1)} custom-call(s32[1]{0:T(128)} %bitcast.4.role_ref, bf16[1024,1024]{1,0:T(8,128)(2,1)} %own, bf16[1024,1024]{1,0:T(8,128)(2,1)} %copy-done.3, bf16[1024,1024]{1,0:T(8,128)(2,1)} %copy-done.4, bf16[512,1024]{1,0:T(8,128)(2,1)} %copy-done.6, bf16[512,1024]{1,0:T(8,128)(2,1)} %collective-permute-done.16.bottom), custom_call_target="tpu_custom_call" | custom-call | flops 1000000 | bytes 2097152 | tf_op jit(solution)/shard_map/pallas_call | solution.py:255
  82.1 2.6 %collective-permute-start.17 = (bf16[1024,1024]{1,0:T(8,128)(2,1)}, bf16[1024,1024]{1,0:T(8,128)(2,1)}, u32[]{:S(2)}, u32[]{:S(2)}) collective-permute-start(bf16[1024,1024]{1,0:T(8,128)(2,1)} %shard_map.77), channel_id=1, source_target_pairs={{0,1},{2,3},{4,5},{6,7},{9,8},{11,10},{13,12},{15,14},{16,17},{18,... | collective-permute-start | bytes 6291464 | tf_op jit(solution)/shard_map/ppermute | solution.py:287
  84.8 2.3 %shard_map.75.refs_0_ = bf16[544,1024]{1,0:T(8,128)(2,1)} custom-call(bf16[136,1024]{1,0:T(8,128)(2,1)} %shard_map.73.refs_0_, bf16[136,1024]{1,0:T(8,128)(2,1)} %collective-permute-done.1.refs_1_, bf16[136,1024]{1,0:T(8,128)(2,1)} %collective-permute-done.2.refs_2_, bf16[136,1024]{1,0:T(8,128)(2,1)} %collective-permute-done.3.refs_3_), custom_call_target="tpu_custom_call" | custom-call | flops 1000000 | bytes 2228224 | tf_op jit(solution)/shard_map/pallas_call | solution.py:88
  87.1 1.6 select_bitcast_fusion
  88.7 3.3 %collective-permute-start = (bf16[4,4,192,128]{3,2,1,0:T(8,128)(2,1)S(1)}, bf16[4,4,192,128]{3,2,1,0:T(8,128)(2,1)S(1)}, u32[]{:S(2)}, u32[]{:S(2)}) collective-permute-start(bf16[4,4,192,128]{3,2,1,0:T(8,128)(2,1)S(1)} %select_bitcast_fusion), channel_id=1, source_target_pairs={{0,32},{32,0},{1,33},{33,1},{2,34},{34,2},{3,35},{35,3},{4,36},{36... | collective-permute-start | bytes 2359304 | tf_op jit(solution)/shard_map/ppermute | solution.py:221
  92.0 3.1 %collective-permute-start.11 = (bf16[544,1024]{1,0:T(8,128)(2,1)S(1)}, bf16[544,1024]{1,0:T(8,128)(2,1)S(1)}, u32[]{:S(2)}, u32[]{:S(2)}) collective-permute-start(bf16[544,1024]{1,0:T(8,128)(2,1)S(1)} %copy-done), channel_id=1, source_target_pairs={{0,24},{8,0},{16,8},{24,16},{1,25},{9,1},{17,9},{25,17},{2,26},{10... | collective-permute-start | bytes 3342344 | tf_op jit(solution)/shard_map/ppermute | solution.py:221
  95.1 1.0 collective-permute-start.18
  96.1 19.7 %collective-permute-done.4.refs_0_ = bf16[544,1024]{1,0:T(8,128)(2,1)S(1)} collective-permute-done((bf16[544,1024]{1,0:T(8,128)(2,1)}, bf16[544,1024]{1,0:T(8,128)(2,1)S(1)}, u32[]{:S(2)}, u32[]{:S(2)}) %collective-permute-start.4) | collective-permute-done | bytes 1114144 | tf_op jit(solution)/shard_map/ppermute | solution.py:221
  115.8 0.0 collective-permute-start.19
  115.9 1.5 bitcast_select_fusion.1
  117.4 0.1 pad_maximum_fusion.q_ref
  117.5 3.2 %collective-permute-done.11.refs_3_ = bf16[544,1024]{1,0:T(8,128)(2,1)S(1)} collective-permute-done((bf16[544,1024]{1,0:T(8,128)(2,1)S(1)}, bf16[544,1024]{1,0:T(8,128)(2,1)S(1)}, u32[]{:S(2)}, u32[]{:S(2)}) %collective-permute-start.11) | collective-permute-done | bytes 1114144 | tf_op jit(solution)/shard_map/ppermute | solution.py:221
  120.8 3.0 %collective-permute-start.12 = (bf16[544,1024]{1,0:T(8,128)(2,1)S(1)}, bf16[544,1024]{1,0:T(8,128)(2,1)S(1)}, u32[]{:S(2)}, u32[]{:S(2)}) collective-permute-start(bf16[544,1024]{1,0:T(8,128)(2,1)S(1)} %collective-permute-done.11.refs_3_), channel_id=1, source_target_pairs={{0,24},{8,0},{16,8},{24,16},{1,25},{9,1},{17,9},{25,17},{2,26},{10... | collective-permute-start | bytes 3342344 | tf_op jit(solution)/shard_map/ppermute | solution.py:221
  123.7 0.2 broadcast_select_fusion.refs_2_.refs_4_
  124.0 10.6 %shard_map.78 = (f32[4,144,1024]{2,1,0:T(8,128)S(1)}, f32[4,8,1024]{2,1,0:T(8,128)S(1)}) custom-call(bf16[8,4,192,128]{3,2,1,0:T(8,128)(2,1)S(1)} %pad_maximum_fusion.q_ref, bf16[544,1024]{1,0:T(8,128)(2,1)S(1)} %copy-done.1, bf16[544,1024]{1,0:T(8,128)(2,1)S(1)} %copy-done, bf16[1024,1024]{1,0:T(8,128)(2,1)S(1)} %broadcast_select_fusion.refs_2_.refs_4_), custom_call_target="tpu_custom_call" | custom-call | flops 8589934592 | bytes 8519680 | tf_op jit(solution)/shard_map/pallas_call | solution.py:178
  134.5 10.1 %collective-permute-done.18.refs_1_ = bf16[544,1024]{1,0:T(8,128)(2,1)S(1)} collective-permute-done((bf16[544,1024]{1,0:T(8,128)(2,1)S(1)}, bf16[544,1024]{1,0:T(8,128)(2,1)S(1)}, u32[]{:S(2)}, u32[]{:S(2)}) %collective-permute-start.18) | collective-permute-done | bytes 1114144 | tf_op jit(solution)/shard_map/ppermute | solution.py:221
  144.6 16.9 %shard_map.79 = (f32[4,144,1024]{2,1,0:T(8,128)S(1)}, f32[4,8,1024]{2,1,0:T(8,128)S(1)}) custom-call(bf16[8,4,192,128]{3,2,1,0:T(8,128)(2,1)S(1)} %pad_maximum_fusion.q_ref, bf16[544,1024]{1,0:T(8,128)(2,1)S(1)} %collective-permute-done.4.refs_0_, bf16[544,1024]{1,0:T(8,128)(2,1)S(1)} %collective-permute-done.18.refs_1_, ...), custom_call_target="tpu_custom_call" | custom-call | flops 17179869184 | bytes 10747904 | tf_op jit(solution)/shard_map/pallas_call | solution.py:178
  161.5 6.0 %collective-permute-done.5.refs_0_ = bf16[544,1024]{1,0:T(8,128)(2,1)S(1)} collective-permute-done((bf16[544,1024]{1,0:T(8,128)(2,1)S(1)}, bf16[544,1024]{1,0:T(8,128)(2,1)S(1)}, u32[]{:S(2)}, u32[]{:S(2)}) %collective-permute-start.5) | collective-permute-done | bytes 1114144 | tf_op jit(solution)/shard_map/ppermute | solution.py:221
  167.5 11.0 %shard_map.80 = bf16[8,128,512]{2,1,0:T(8,128)(2,1)S(1)} custom-call(bf16[8,4,192,128]{3,2,1,0:T(8,128)(2,1)S(1)} %pad_maximum_fusion.q_ref, bf16[544,1024]{1,0:T(8,128)(2,1)S(1)} %collective-permute-done.5.refs_0_, bf16[544,1024]{1,0:T(8,128)(2,1)S(1)} %collective-permute-done.12.refs_1_, bf16[1024,1024]{1,0:T(8,128)(2,1)S(1)} %broadcast_select_fusion.refs_2_.refs_4_, ...), custom_call_target="tpu_custom_call" | custom-call | flops 8589934592 | bytes 8519680 | tf_op jit(solution)/shard_map/pallas_call | solution.py:178
  178.5 20.7 %all_to_all.10.heads_ref = bf16[8,128,512]{2,1,0:T(8,128)(2,1)} all-to-all(bf16[8,128,512]{2,1,0:T(8,128)(2,1)S(1)} %shard_map.80), channel_id=1, replica_groups=mesh['zh'=4,'zl'=2,'y'=4,'x'=4,'core'=2] {'zl','y'}, dimensions={0} | all-to-all | bytes 2097152 | tf_op jit(solution)/shard_map/all_to_all | solution.py:330
  199.2 3.4 %shard_map.81 = bf16[128,4096]{1,0:T(8,128)(2,1)} custom-call(bf16[8,128,512]{2,1,0:T(8,128)(2,1)} %all_to_all.10.heads_ref, bf16[128,4096]{1,0:T(8,128)(2,1)} %gate_ref.1, f32[1,4096]{1,0:T(1,128)} %bitcast.29), custom_call_target="tpu_custom_call" | custom-call | flops 10000000 | bytes 3145728 | tf_op jit(solution)/shard_map/pallas_call | solution.py:331
  (35 shorter events, 0.1 us)
Async XLA Ops:
  3.0 33.9 %copy-start.5 = (bf16[136,1024]{1,0:T(8,128)(2,1)S(1)}, bf16[136,1024]{1,0:T(8,128)(2,1)}, u32[]{:S(2)}) copy-start(bf16[136,1024]{1,0:T(8,128)(2,1)} %shard_map.73.refs_0_) | copy-start | bytes 835588
  3.0 2.2 %collective-permute-start.13 = (bf16[1024,1024]{1,0:T(8,128)(2,1)}, bf16[1024,1024]{1,0:T(8,128)(2,1)S(1)}, u32[]{:S(2)}, u32[]{:S(2)}) collective-permute-start(bf16[1024,1024]{1,0:T(8,128)(2,1)} %own), channel_id=1, source_target_pairs={{0,2},{9,11},{18,20},{27,29},{36,38},{45,47},{54,48},{63,57},{64,6... | collective-permute-start | bytes 6291464 | tf_op jit(solution)/shard_map/ppermute | solution.py:277
  3.9 29.4 %collective-permute-start.14 = (bf16[1024,1024]{1,0:T(8,128)(2,1)}, bf16[1024,1024]{1,0:T(8,128)(2,1)S(1)}, u32[]{:S(2)}, u32[]{:S(2)}) collective-permute-start(bf16[1024,1024]{1,0:T(8,128)(2,1)} %own), channel_id=1, source_target_pairs={{0,6},{9,15},{18,16},{27,25},{36,34},{45,43},{54,52},{63,61},{64,7... | collective-permute-start | bytes 6291464 | tf_op jit(solution)/shard_map/ppermute | solution.py:278
  5.2 28.9 %copy-start.3 = (bf16[1024,1024]{1,0:T(8,128)(2,1)}, bf16[1024,1024]{1,0:T(8,128)(2,1)S(1)}, u32[]{:S(2)}) copy-start(bf16[1024,1024]{1,0:T(8,128)(2,1)S(1)} %collective-permute-done.13.right) | copy-start | bytes 6291460
  33.2 1.3 copy-start.4
  33.3 44.8 %collective-permute-start.15 = (bf16[512,1024]{1,0:T(8,128)(2,1)S(1)}, bf16[512,1024]{1,0:T(8,128)(2,1)S(1)}, u32[]{:S(2)}, u32[]{:S(2)}) collective-permute-start(bf16[512,1024]{1,0:T(8,128)(2,1)S(1)} %slice.24), channel_id=1, source_target_pairs={{2,4},{11,13},{20,22},{29,31},{38,32},{47,41},{48,50},{57,59},{66,... | collective-permute-start | bytes 3145736 | tf_op jit(solution)/shard_map/ppermute | solution.py:280
  34.6 43.6 %collective-permute-start.16 = (bf16[512,1024]{1,0:T(8,128)(2,1)S(1)}, bf16[512,1024]{1,0:T(8,128)(2,1)}, u32[]{:S(2)}, u32[]{:S(2)}) collective-permute-start(bf16[512,1024]{1,0:T(8,128)(2,1)S(1)} %slice.25), channel_id=1, source_target_pairs={{6,4},{15,13},{16,22},{25,31},{34,32},{43,41},{52,50},{61,59},{70,... | collective-permute-start | bytes 3145736 | tf_op jit(solution)/shard_map/ppermute | solution.py:281
  36.8 6.7 %collective-permute-start.1 = (bf16[136,1024]{1,0:T(8,128)(2,1)S(1)}, bf16[136,1024]{1,0:T(8,128)(2,1)}, u32[]{:S(2)}, u32[]{:S(2)}) collective-permute-start(bf16[136,1024]{1,0:T(8,128)(2,1)S(1)} %copy-done.5), channel_id=1, source_target_pairs={{0,32},{32,64},{64,96},{96,128},{128,160},{160,192},{192,224},{224... | collective-permute-start | bytes 835592 | tf_op jit(solution)/shard_map/ppermute | solution.py:221
  36.8 9.7 %collective-permute-start.2 = (bf16[136,1024]{1,0:T(8,128)(2,1)S(1)}, bf16[136,1024]{1,0:T(8,128)(2,1)}, u32[]{:S(2)}, u32[]{:S(2)}) collective-permute-start(bf16[136,1024]{1,0:T(8,128)(2,1)S(1)} %copy-done.5), channel_id=1, source_target_pairs={{0,224},{32,0},{64,32},{96,64},{128,96},{160,128},{192,160},{224,1... | collective-permute-start | bytes 835592 | tf_op jit(solution)/shard_map/ppermute | solution.py:221
  43.5 10.6 %collective-permute-start.3 = (bf16[136,1024]{1,0:T(8,128)(2,1)}, bf16[136,1024]{1,0:T(8,128)(2,1)}, u32[]{:S(2)}, u32[]{:S(2)}) collective-permute-start(bf16[136,1024]{1,0:T(8,128)(2,1)} %collective-permute-done.1.refs_1_), channel_id=1, source_target_pairs={{0,32},{32,64},{64,96},{96,128},{128,160},{160,192},{192,224},{224... | collective-permute-start | bytes 835592 | tf_op jit(solution)/shard_map/ppermute | solution.py:221
  46.5 10.9 %collective-permute-start.6 = (bf16[136,1024]{1,0:T(8,128)(2,1)}, bf16[136,1024]{1,0:T(8,128)(2,1)}, u32[]{:S(2)}, u32[]{:S(2)}) collective-permute-start(bf16[136,1024]{1,0:T(8,128)(2,1)} %collective-permute-done.2.refs_2_), channel_id=1, source_target_pairs={{0,224},{32,0},{64,32},{96,64},{128,96},{160,128},{192,160},{224,1... | collective-permute-start | bytes 835592 | tf_op jit(solution)/shard_map/ppermute | solution.py:221
  49.7 37.4 %all-to-all-start = ((bf16[4,2,4,192,128]{4,3,2,1,0:T(8,128)(2,1)}), bf16[4,2,4,192,128]{4,3,2,1,0:T(8,128)(2,1)}, u32[]{:S(2)}, u32[]{:S(2)}) async-start(bf16[4,2,4,192,128]{4,3,2,1,0:T(8,128)(2,1)} %shard_map.74), calls=%async_computation | async-start | bytes 3145728 | tf_op jit(solution)/shard_map/all_to_all | solution.py:307
  54.1 9.1 %collective-permute-start.7 = (bf16[136,1024]{1,0:T(8,128)(2,1)}, bf16[136,1024]{1,0:T(8,128)(2,1)S(1)}, u32[]{:S(2)}, u32[]{:S(2)}) collective-permute-start(bf16[136,1024]{1,0:T(8,128)(2,1)} %collective-permute-done.3.refs_3_), channel_id=1, source_target_pairs={{0,32},{32,64},{64,96},{96,128},{128,160},{160,192},{192,224},{224... | collective-permute-start | bytes 835592 | tf_op jit(solution)/shard_map/ppermute | solution.py:221
  57.4 9.7 %collective-permute-start.8 = (bf16[136,1024]{1,0:T(8,128)(2,1)}, bf16[136,1024]{1,0:T(8,128)(2,1)S(1)}, u32[]{:S(2)}, u32[]{:S(2)}) collective-permute-start(bf16[136,1024]{1,0:T(8,128)(2,1)} %collective-permute-done.6.refs_0_), channel_id=1, source_target_pairs={{0,224},{32,0},{64,32},{96,64},{128,96},{160,128},{192,160},{224,1... | collective-permute-start | bytes 835592 | tf_op jit(solution)/shard_map/ppermute | solution.py:221
  63.1 12.0 %copy-start.7 = (bf16[136,1024]{1,0:T(8,128)(2,1)}, bf16[136,1024]{1,0:T(8,128)(2,1)S(1)}, u32[]{:S(2)}) copy-start(bf16[136,1024]{1,0:T(8,128)(2,1)S(1)} %collective-permute-done.7.refs_1_) | copy-start | bytes 835588
  63.9 11.3 %collective-permute-start.9 = (bf16[72,1024]{1,0:T(8,128)(2,1)}, bf16[72,1024]{1,0:T(8,128)(2,1)}, u32[]{:S(2)}, u32[]{:S(2)}) collective-permute-start(bf16[72,1024]{1,0:T(8,128)(2,1)} %slice.28), channel_id=1, source_target_pairs={{0,32},{32,64},{64,96},{96,128},{128,160},{160,192},{192,224},{224... | collective-permute-start | bytes 442376 | tf_op jit(solution)/shard_map/ppermute | solution.py:221
  67.0 0.7 copy-start.8
  68.4 6.7 %collective-permute-start.10 = (bf16[64,1024]{1,0:T(8,128)(2,1)}, bf16[64,1024]{1,0:T(8,128)(2,1)S(1)}, u32[]{:S(2)}, u32[]{:S(2)}) collective-permute-start(bf16[64,1024]{1,0:T(8,128)(2,1)} %slice.29), channel_id=1, source_target_pairs={{0,224},{32,0},{64,32},{96,64},{128,96},{160,128},{192,160},{224,1... | collective-permute-start | bytes 393224 | tf_op jit(solution)/shard_map/ppermute | solution.py:221
  75.2 0.7 copy-start.9
  78.2 1.0 copy-start.6
  82.1 41.6 %collective-permute-start.17 = (bf16[1024,1024]{1,0:T(8,128)(2,1)}, bf16[1024,1024]{1,0:T(8,128)(2,1)}, u32[]{:S(2)}, u32[]{:S(2)}) collective-permute-start(bf16[1024,1024]{1,0:T(8,128)(2,1)} %shard_map.77), channel_id=1, source_target_pairs={{0,1},{2,3},{4,5},{6,7},{9,8},{11,10},{13,12},{15,14},{16,17},{18,... | collective-permute-start | bytes 6291464 | tf_op jit(solution)/shard_map/ppermute | solution.py:287
  87.1 5.0 %copy-start = (bf16[544,1024]{1,0:T(8,128)(2,1)S(1)}, bf16[544,1024]{1,0:T(8,128)(2,1)}, u32[]{:S(2)}) copy-start(bf16[544,1024]{1,0:T(8,128)(2,1)} %shard_map.76.refs_1_) | copy-start | bytes 3342340
  87.1 8.0 %copy-start.1 = (bf16[544,1024]{1,0:T(8,128)(2,1)S(1)}, bf16[544,1024]{1,0:T(8,128)(2,1)}, u32[]{:S(2)}) copy-start(bf16[544,1024]{1,0:T(8,128)(2,1)} %shard_map.75.refs_0_) | copy-start | bytes 3342340
  87.1 28.8 %collective-permute-start.4 = (bf16[544,1024]{1,0:T(8,128)(2,1)}, bf16[544,1024]{1,0:T(8,128)(2,1)S(1)}, u32[]{:S(2)}, u32[]{:S(2)}) collective-permute-start(bf16[544,1024]{1,0:T(8,128)(2,1)} %shard_map.75.refs_0_), channel_id=1, source_target_pairs={{0,8},{8,16},{16,24},{24,0},{1,9},{9,17},{17,25},{25,1},{2,10},{10... | collective-permute-start | bytes 3342344 | tf_op jit(solution)/shard_map/ppermute | solution.py:221
  88.7 27.1 %collective-permute-start = (bf16[4,4,192,128]{3,2,1,0:T(8,128)(2,1)S(1)}, bf16[4,4,192,128]{3,2,1,0:T(8,128)(2,1)S(1)}, u32[]{:S(2)}, u32[]{:S(2)}) collective-permute-start(bf16[4,4,192,128]{3,2,1,0:T(8,128)(2,1)S(1)} %select_bitcast_fusion), channel_id=1, source_target_pairs={{0,32},{32,0},{1,33},{33,1},{2,34},{34,2},{3,35},{35,3},{4,36},{36... | collective-permute-start | bytes 2359304 | tf_op jit(solution)/shard_map/ppermute | solution.py:221
  92.0 28.7 %collective-permute-start.11 = (bf16[544,1024]{1,0:T(8,128)(2,1)S(1)}, bf16[544,1024]{1,0:T(8,128)(2,1)S(1)}, u32[]{:S(2)}, u32[]{:S(2)}) collective-permute-start(bf16[544,1024]{1,0:T(8,128)(2,1)S(1)} %copy-done), channel_id=1, source_target_pairs={{0,24},{8,0},{16,8},{24,16},{1,25},{9,1},{17,9},{25,17},{2,26},{10... | collective-permute-start | bytes 3342344 | tf_op jit(solution)/shard_map/ppermute | solution.py:221
  95.1 49.6 %collective-permute-start.18 = (bf16[544,1024]{1,0:T(8,128)(2,1)S(1)}, bf16[544,1024]{1,0:T(8,128)(2,1)S(1)}, u32[]{:S(2)}, u32[]{:S(2)}) collective-permute-start(bf16[544,1024]{1,0:T(8,128)(2,1)S(1)} %copy-done.1), channel_id=1, source_target_pairs={{0,24},{8,0},{16,8},{24,16},{1,25},{9,1},{17,9},{25,17},{2,26},{10... | collective-permute-start | bytes 3342344 | tf_op jit(solution)/shard_map/ppermute | solution.py:221
  115.8 28.8 %collective-permute-start.19 = (bf16[544,1024]{1,0:T(8,128)(2,1)S(1)}, bf16[544,1024]{1,0:T(8,128)(2,1)S(1)}, u32[]{:S(2)}, u32[]{:S(2)}) collective-permute-start(bf16[544,1024]{1,0:T(8,128)(2,1)S(1)} %copy-done), channel_id=1, source_target_pairs={{0,8},{8,16},{16,24},{24,0},{1,9},{9,17},{17,25},{25,1},{2,10},{10... | collective-permute-start | bytes 3342344 | tf_op jit(solution)/shard_map/ppermute | solution.py:221
  115.8 51.7 %collective-permute-start.5 = (bf16[544,1024]{1,0:T(8,128)(2,1)S(1)}, bf16[544,1024]{1,0:T(8,128)(2,1)S(1)}, u32[]{:S(2)}, u32[]{:S(2)}) collective-permute-start(bf16[544,1024]{1,0:T(8,128)(2,1)S(1)} %collective-permute-done.4.refs_0_), channel_id=1, source_target_pairs={{0,8},{8,16},{16,24},{24,0},{1,9},{9,17},{17,25},{25,1},{2,10},{10... | collective-permute-start | bytes 3342344 | tf_op jit(solution)/shard_map/ppermute | solution.py:221
  117.4 6.4 %copy-start.2 = (bf16[1024,1024]{1,0:T(8,128)(2,1)S(1)}, bf16[1024,1024]{1,0:T(8,128)(2,1)}, u32[]{:S(2)}) copy-start(bf16[1024,1024]{1,0:T(8,128)(2,1)} %shard_map.77) | copy-start | bytes 6291460
  120.8 46.7 %collective-permute-start.12 = (bf16[544,1024]{1,0:T(8,128)(2,1)S(1)}, bf16[544,1024]{1,0:T(8,128)(2,1)S(1)}, u32[]{:S(2)}, u32[]{:S(2)}) collective-permute-start(bf16[544,1024]{1,0:T(8,128)(2,1)S(1)} %collective-permute-done.11.refs_3_), channel_id=1, source_target_pairs={{0,24},{8,0},{16,8},{24,16},{1,25},{9,1},{17,9},{25,17},{2,26},{10... | collective-permute-start | bytes 3342344 | tf_op jit(solution)/shard_map/ppermute | solution.py:221

commit v4 on v3

--- a/solution.py
+++ b/solution.py
@@ -162,9 +162,10 @@
             out_ref[source] = (part[:VDIM] / part[VDIM : VDIM + 1]).T.astype(BF16)
 
 
-def attention(queries, pieces, weight, state=(), ends=False, bq=512, bk=1024):
+def attention(queries, pieces, weight, state=(), ends=False, bq=512):
     sizes = tuple(p.shape[0] for p in pieces)
     keys = sum(sizes) // BLOCK * OWN
+    bk = 1024 if keys % 1536 else 1536
     state_shapes = (PER, VDIM + 16, ROWS), (PER, 8, ROWS)
     state_specs = [pl.BlockSpec((1, *shape[1:]), lambda h: (h, 0, 0)) for shape in state_shapes]
     if ends:
@@ -324,8 +325,7 @@
     beside0 = [shifted(first, "y", 1), shifted(first, "y", -1)]
     beside1 = [shifted(second, "y", 1), shifted(second, "y", -1)]
     opposite = [shifted(beside0[0], "y", 1), shifted(beside1[1], "y", -1)]
-    state = attention(head_queries, [first, second], weight)
-    state = attention(head_queries, beside0 + beside1, weight, state)
+    state = attention(head_queries, [first, second, *beside0, *beside1], weight)
     heads_out = attention(head_queries, opposite, weight, state, ends=True)
     heads_out = lax.all_to_all(heads_out, ("zl", "y"), 0, 0, tiled=True)
     return call(

time: 203 us -> 203 us (level)
  waiting for transfers between devices: 84.8 us -> 89.4 us
  Pallas kernels: 54.6 us -> 51.4 us
    ppermute x15, waiting for transfers between devices: 56.7 us -> 61.3 us  [shifted(): lax.ppermute(value, axis, [(i, (i + by) % length) for i in range(length)])]
    pallas_call x3 -> x2, Pallas kernels: 38.4 us -> 35.3 us  [attention(): pl.pallas_call(functools.partial(attention_kernel, sizes, bq, bk, not sta...]
  transfers between devices with their start and end apart: 21 -> 21, of which waited for: 9 -> 8; matrix products, arithmetic and copies ran while one was open for 2% -> 2% of each run, Pallas kernels for 19% -> 17%
where the time goes in v4:
time: 203 us
  waiting for transfers between devices  89.4 us (44%)
  Pallas kernels  51.4 us (25%)
  starting transfers between devices  33.6 us (17%)
  blocking collectives  19.5 us (10%)
  other arithmetic  4.46 us (2%)
  local copies, waits for them, and re-layouts  4.32 us (2%)
    ppermute x15, waiting for transfers between devices, shifted(): lax.ppermute(value, axis, [(i, (i + by) % length) for i in range(length)])  61.3 us
    pallas_call x2, Pallas kernels, attention(): pl.pallas_call(functools.partial(attention_kernel, sizes, bq, bk, not sta...  35.3 us
    ppermute x1, waiting for transfers between devices, shard_of_group(): left = lax.ppermute(weight, EVERY, one_way(-1))  28 us
    ppermute x15, starting transfers between devices, shifted(): lax.ppermute(value, axis, [(i, (i + by) % length) for i in range(length)])  21.4 us
    all_to_all x1, blocking collectives, per_device(): heads_out = lax.all_to_all(heads_out, ('zl', 'y'), 0, 0, tiled=True)  19.5 us
    pallas_call x2, Pallas kernels, joined(): return call(joined_kernel, (rows, RANK), 10 ** 6, 4 * rows * RANK)(*pieces)  4.61 us
    all_to_all x1, starting transfers between devices, per_device(): head_queries = lax.all_to_all(head_queries, 'y', 0, 0, tiled=True)  4.36 us
  transfers between devices with their start and end apart: 21, of which 8 were waited for; matrix products, arithmetic and copies ran while one was open for 2% of the time, Pallas kernels for 17%

profile of v4, /device:TPU:70, one launch (start us, length us, event | category | flops | bytes accessed | tf_op | source)
XLA Modules:
  0.0 202.9 jit_solution(7594417656696617131)
XLA Ops:
  0.0 1.0 multiply_sine_fusion
  1.0 2.0 shard_map.73.refs_0_
  3.0 0.9 collective-permute-start.13
  3.9 1.3 collective-permute-start.14
  5.2 0.0 collective-permute-done.13.right
  5.2 28.0 %collective-permute-done.14.left = bf16[1024,1024]{1,0:T(8,128)(2,1)S(1)} collective-permute-done((bf16[1024,1024]{1,0:T(8,128)(2,1)}, bf16[1024,1024]{1,0:T(8,128)(2,1)S(1)}, u32[]{:S(2)}, u32[]{:S(2)}) %collective-permute-start.14) | collective-permute-done | bytes 2097184 | tf_op jit(solution)/shard_map/ppermute | solution.py:279
  33.2 0.1 slice.24
  33.3 0.7 collective-permute-start.15
  34.1 0.1 slice.25
  34.1 0.4 copy-done.4
  34.6 2.3 %collective-permute-start.16 = (bf16[512,1024]{1,0:T(8,128)(2,1)S(1)}, bf16[512,1024]{1,0:T(8,128)(2,1)}, u32[]{:S(2)}, u32[]{:S(2)}) collective-permute-start(bf16[512,1024]{1,0:T(8,128)(2,1)S(1)} %slice.25), channel_id=1, source_target_pairs={{6,4},{15,13},{16,22},{25,31},{34,32},{43,41},{52,50},{61,59},{70,... | collective-permute-start | bytes 3145736 | tf_op jit(solution)/shard_map/ppermute | solution.py:282
  36.8 0.0 collective-permute-start.1
  36.8 2.0 collective-permute-start.2
  38.9 4.6 %collective-permute-done.1.refs_1_ = bf16[136,1024]{1,0:T(8,128)(2,1)} collective-permute-done((bf16[136,1024]{1,0:T(8,128)(2,1)S(1)}, bf16[136,1024]{1,0:T(8,128)(2,1)}, u32[]{:S(2)}, u32[]{:S(2)}) %collective-permute-start.1) | collective-permute-done | bytes 278560 | tf_op jit(solution)/shard_map/ppermute | solution.py:222
  43.5 2.5 %collective-permute-start.3 = (bf16[136,1024]{1,0:T(8,128)(2,1)}, bf16[136,1024]{1,0:T(8,128)(2,1)}, u32[]{:S(2)}, u32[]{:S(2)}) collective-permute-start(bf16[136,1024]{1,0:T(8,128)(2,1)} %collective-permute-done.1.refs_1_), channel_id=1, source_target_pairs={{0,32},{32,64},{64,96},{96,128},{128,160},{160,192},{192,224},{224... | collective-permute-start | bytes 835592 | tf_op jit(solution)/shard_map/ppermute | solution.py:222
  46.0 0.6 collective-permute-done.2.refs_2_
  46.5 3.2 %shard_map.74 = bf16[4,2,4,192,128]{4,3,2,1,0:T(8,128)(2,1)} custom-call(bf16[128,6144]{1,0:T(8,128)(2,1)} %q_ref, f32[128,32]{1,0:T(8,128)} %get-tuple-element.26.cos_ref, f32[128,32]{1,0:T(8,128)} %get-tuple-element.25.sin_ref), custom_call_target="tpu_custom_call" | custom-call | flops 10000000 | bytes 3145728 | tf_op jit(solution)/shard_map/pallas_call | solution.py:303
  49.7 4.4 %all-to-all-start = ((bf16[4,2,4,192,128]{4,3,2,1,0:T(8,128)(2,1)}), bf16[4,2,4,192,128]{4,3,2,1,0:T(8,128)(2,1)}, u32[]{:S(2)}, u32[]{:S(2)}) async-start(bf16[4,2,4,192,128]{4,3,2,1,0:T(8,128)(2,1)} %shard_map.74), calls=%async_computation | async-start | bytes 3145728 | tf_op jit(solution)/shard_map/all_to_all | solution.py:308
  54.1 0.0 collective-permute-done.3.refs_3_
  54.1 3.3 %collective-permute-start.7 = (bf16[136,1024]{1,0:T(8,128)(2,1)}, bf16[136,1024]{1,0:T(8,128)(2,1)S(1)}, u32[]{:S(2)}, u32[]{:S(2)}) collective-permute-start(bf16[136,1024]{1,0:T(8,128)(2,1)} %collective-permute-done.3.refs_3_), channel_id=1, source_target_pairs={{0,32},{32,64},{64,96},{96,128},{128,160},{160,192},{192,224},{224... | collective-permute-start | bytes 835592 | tf_op jit(solution)/shard_map/ppermute | solution.py:222
  57.4 5.8 %collective-permute-done.7.refs_1_ = bf16[136,1024]{1,0:T(8,128)(2,1)S(1)} collective-permute-done((bf16[136,1024]{1,0:T(8,128)(2,1)}, bf16[136,1024]{1,0:T(8,128)(2,1)S(1)}, u32[]{:S(2)}, u32[]{:S(2)}) %collective-permute-start.7) | collective-permute-done | bytes 278560 | tf_op jit(solution)/shard_map/ppermute | solution.py:222
  63.2 0.7 slice.28
  63.9 3.2 %collective-permute-start.9 = (bf16[72,1024]{1,0:T(8,128)(2,1)}, bf16[72,1024]{1,0:T(8,128)(2,1)}, u32[]{:S(2)}, u32[]{:S(2)}) collective-permute-start(bf16[72,1024]{1,0:T(8,128)(2,1)} %slice.28), channel_id=1, source_target_pairs={{0,32},{32,64},{64,96},{96,128},{128,160},{160,192},{192,224},{224... | collective-permute-start | bytes 442376 | tf_op jit(solution)/shard_map/ppermute | solution.py:222
  67.1 0.7 copy-done.8
  67.8 0.7 slice.29
  68.5 6.7 %collective-permute-done.10.refs_4_ = bf16[64,1024]{1,0:T(8,128)(2,1)S(1)} collective-permute-done((bf16[64,1024]{1,0:T(8,128)(2,1)}, bf16[64,1024]{1,0:T(8,128)(2,1)S(1)}, u32[]{:S(2)}, u32[]{:S(2)}) %collective-permute-start.10) | collective-permute-done | bytes 131104 | tf_op jit(solution)/shard_map/ppermute | solution.py:222
  75.2 0.6 copy-done.9
  75.9 2.3 %shard_map.76.refs_1_ = bf16[544,1024]{1,0:T(8,128)(2,1)} custom-call(bf16[136,1024]{1,0:T(8,128)(2,1)} %collective-permute-done.6.refs_0_, bf16[136,1024]{1,0:T(8,128)(2,1)} %copy-done.7, bf16[136,1024]{1,0:T(8,128)(2,1)} %copy-done.8, bf16[72,1024]{1,0:T(8,128)(2,1)} %collective-permute-done.9.refs_3_, bf16[64,1024]{1,0:T(8,128)(2,1)} %copy-done.9), custom_call_target="tpu_custom_call" | custom-call | flops 1000000 | bytes 2228224 | tf_op jit(solution)/shard_map/pallas_call | solution.py:88
  78.2 1.0 copy-done.6
  79.1 3.0 %shard_map.77 = bf16[1024,1024]{1,0:T(8,128)(2,1)} custom-call(s32[1]{0:T(128)} %bitcast.4.role_ref, bf16[1024,1024]{1,0:T(8,128)(2,1)} %own, bf16[1024,1024]{1,0:T(8,128)(2,1)} %copy-done.3, bf16[1024,1024]{1,0:T(8,128)(2,1)} %copy-done.4, bf16[512,1024]{1,0:T(8,128)(2,1)} %copy-done.6, bf16[512,1024]{1,0:T(8,128)(2,1)} %collective-permute-done.16.bottom), custom_call_target="tpu_custom_call" | custom-call | flops 1000000 | bytes 2097152 | tf_op jit(solution)/shard_map/pallas_call | solution.py:256
  82.1 2.6 %collective-permute-start.17 = (bf16[1024,1024]{1,0:T(8,128)(2,1)}, bf16[1024,1024]{1,0:T(8,128)(2,1)}, u32[]{:S(2)}, u32[]{:S(2)}) collective-permute-start(bf16[1024,1024]{1,0:T(8,128)(2,1)} %shard_map.77), channel_id=1, source_target_pairs={{0,1},{2,3},{4,5},{6,7},{9,8},{11,10},{13,12},{15,14},{16,17},{18,... | collective-permute-start | bytes 6291464 | tf_op jit(solution)/shard_map/ppermute | solution.py:288
  84.8 2.3 %shard_map.75.refs_0_ = bf16[544,1024]{1,0:T(8,128)(2,1)} custom-call(bf16[136,1024]{1,0:T(8,128)(2,1)} %shard_map.73.refs_0_, bf16[136,1024]{1,0:T(8,128)(2,1)} %collective-permute-done.1.refs_1_, bf16[136,1024]{1,0:T(8,128)(2,1)} %collective-permute-done.2.refs_2_, bf16[136,1024]{1,0:T(8,128)(2,1)} %collective-permute-done.3.refs_3_), custom_call_target="tpu_custom_call" | custom-call | flops 1000000 | bytes 2228224 | tf_op jit(solution)/shard_map/pallas_call | solution.py:88
  87.1 1.6 select_bitcast_fusion
  88.7 3.3 %collective-permute-start = (bf16[4,4,192,128]{3,2,1,0:T(8,128)(2,1)S(1)}, bf16[4,4,192,128]{3,2,1,0:T(8,128)(2,1)S(1)}, u32[]{:S(2)}, u32[]{:S(2)}) collective-permute-start(bf16[4,4,192,128]{3,2,1,0:T(8,128)(2,1)S(1)} %select_bitcast_fusion), channel_id=1, source_target_pairs={{0,32},{32,0},{1,33},{33,1},{2,34},{34,2},{3,35},{35,3},{4,36},{36... | collective-permute-start | bytes 2359304 | tf_op jit(solution)/shard_map/ppermute | solution.py:222
  92.0 3.1 %collective-permute-start.11 = (bf16[544,1024]{1,0:T(8,128)(2,1)S(1)}, bf16[544,1024]{1,0:T(8,128)(2,1)S(1)}, u32[]{:S(2)}, u32[]{:S(2)}) collective-permute-start(bf16[544,1024]{1,0:T(8,128)(2,1)S(1)} %copy-done), channel_id=1, source_target_pairs={{0,24},{8,0},{16,8},{24,16},{1,25},{9,1},{17,9},{25,17},{2,26},{10... | collective-permute-start | bytes 3342344 | tf_op jit(solution)/shard_map/ppermute | solution.py:222
  95.1 1.0 collective-permute-start.18
  96.2 19.7 %collective-permute-done.4.refs_2_ = bf16[544,1024]{1,0:T(8,128)(2,1)S(1)} collective-permute-done((bf16[544,1024]{1,0:T(8,128)(2,1)}, bf16[544,1024]{1,0:T(8,128)(2,1)S(1)}, u32[]{:S(2)}, u32[]{:S(2)}) %collective-permute-start.4) | collective-permute-done | bytes 1114144 | tf_op jit(solution)/shard_map/ppermute | solution.py:222
  115.9 0.0 collective-permute-start.19
  115.9 1.5 bitcast_select_fusion.1
  117.4 0.1 pad_maximum_fusion.q_ref
  117.5 3.2 %collective-permute-done.11.refs_5_ = bf16[544,1024]{1,0:T(8,128)(2,1)S(1)} collective-permute-done((bf16[544,1024]{1,0:T(8,128)(2,1)S(1)}, bf16[544,1024]{1,0:T(8,128)(2,1)S(1)}, u32[]{:S(2)}, u32[]{:S(2)}) %collective-permute-start.11) | collective-permute-done | bytes 1114144 | tf_op jit(solution)/shard_map/ppermute | solution.py:222
  120.8 3.0 %collective-permute-start.12 = (bf16[544,1024]{1,0:T(8,128)(2,1)S(1)}, bf16[544,1024]{1,0:T(8,128)(2,1)S(1)}, u32[]{:S(2)}, u32[]{:S(2)}) collective-permute-start(bf16[544,1024]{1,0:T(8,128)(2,1)S(1)} %collective-permute-done.11.refs_5_), channel_id=1, source_target_pairs={{0,24},{8,0},{16,8},{24,16},{1,25},{9,1},{17,9},{25,17},{2,26},{10... | collective-permute-start | bytes 3342344 | tf_op jit(solution)/shard_map/ppermute | solution.py:222
  123.8 0.2 broadcast_select_fusion.refs_6_.refs_2_
  124.0 20.7 %collective-permute-done.18.refs_3_ = bf16[544,1024]{1,0:T(8,128)(2,1)S(1)} collective-permute-done((bf16[544,1024]{1,0:T(8,128)(2,1)S(1)}, bf16[544,1024]{1,0:T(8,128)(2,1)S(1)}, u32[]{:S(2)}, u32[]{:S(2)}) %collective-permute-start.18) | collective-permute-done | bytes 1114144 | tf_op jit(solution)/shard_map/ppermute | solution.py:222
  144.7 24.2 %shard_map.78 = (f32[4,144,1024]{2,1,0:T(8,128)S(1)}, f32[4,8,1024]{2,1,0:T(8,128)S(1)}) custom-call(bf16[8,4,192,128]{3,2,1,0:T(8,128)(2,1)S(1)} %pad_maximum_fusion.q_ref, bf16[544,1024]{1,0:T(8,128)(2,1)S(1)} %copy-done.1, bf16[544,1024]{1,0:T(8,128)(2,1)S(1)} %copy-done, bf16[544,1024]{1,0:T(8,128)(2,1)S(1)} %collective-permute-done.4.refs_2_, ...), custom_call_target="tpu_custom_call" | custom-call | flops 25769803776 | bytes 12976128 | tf_op jit(solution)/shard_map/pallas_call | solution.py:179
  168.9 11.0 %shard_map.79 = bf16[8,128,512]{2,1,0:T(8,128)(2,1)S(1)} custom-call(bf16[8,4,192,128]{3,2,1,0:T(8,128)(2,1)S(1)} %pad_maximum_fusion.q_ref, bf16[544,1024]{1,0:T(8,128)(2,1)S(1)} %collective-permute-done.5.refs_0_, bf16[544,1024]{1,0:T(8,128)(2,1)S(1)} %collective-permute-done.12.refs_1_, bf16[1024,1024]{1,0:T(8,128)(2,1)S(1)} %broadcast_select_fusion.refs_6_.refs_2_, ...), custom_call_target="tpu_custom_call" | custom-call | flops 8589934592 | bytes 8519680 | tf_op jit(solution)/shard_map/pallas_call | solution.py:179
  180.0 19.5 %all_to_all.10.heads_ref = bf16[8,128,512]{2,1,0:T(8,128)(2,1)} all-to-all(bf16[8,128,512]{2,1,0:T(8,128)(2,1)S(1)} %shard_map.79), channel_id=1, replica_groups=mesh['zh'=4,'zl'=2,'y'=4,'x'=4,'core'=2] {'zl','y'}, dimensions={0} | all-to-all | bytes 2097152 | tf_op jit(solution)/shard_map/all_to_all | solution.py:330
  199.5 3.4 %shard_map.80 = bf16[128,4096]{1,0:T(8,128)(2,1)} custom-call(bf16[8,128,512]{2,1,0:T(8,128)(2,1)} %all_to_all.10.heads_ref, bf16[128,4096]{1,0:T(8,128)(2,1)} %gate_ref.1, f32[1,4096]{1,0:T(1,128)} %bitcast.29), custom_call_target="tpu_custom_call" | custom-call | flops 10000000 | bytes 3145728 | tf_op jit(solution)/shard_map/pallas_call | solution.py:331
  (34 shorter events, 0.1 us)
Async XLA Ops:
  3.0 33.9 %copy-start.5 = (bf16[136,1024]{1,0:T(8,128)(2,1)S(1)}, bf16[136,1024]{1,0:T(8,128)(2,1)}, u32[]{:S(2)}) copy-start(bf16[136,1024]{1,0:T(8,128)(2,1)} %shard_map.73.refs_0_) | copy-start | bytes 835588
  3.0 2.2 %collective-permute-start.13 = (bf16[1024,1024]{1,0:T(8,128)(2,1)}, bf16[1024,1024]{1,0:T(8,128)(2,1)S(1)}, u32[]{:S(2)}, u32[]{:S(2)}) collective-permute-start(bf16[1024,1024]{1,0:T(8,128)(2,1)} %own), channel_id=1, source_target_pairs={{0,2},{9,11},{18,20},{27,29},{36,38},{45,47},{54,48},{63,57},{64,6... | collective-permute-start | bytes 6291464 | tf_op jit(solution)/shard_map/ppermute | solution.py:278
  3.9 29.4 %collective-permute-start.14 = (bf16[1024,1024]{1,0:T(8,128)(2,1)}, bf16[1024,1024]{1,0:T(8,128)(2,1)S(1)}, u32[]{:S(2)}, u32[]{:S(2)}) collective-permute-start(bf16[1024,1024]{1,0:T(8,128)(2,1)} %own), channel_id=1, source_target_pairs={{0,6},{9,15},{18,16},{27,25},{36,34},{45,43},{54,52},{63,61},{64,7... | collective-permute-start | bytes 6291464 | tf_op jit(solution)/shard_map/ppermute | solution.py:279
  5.2 28.9 %copy-start.3 = (bf16[1024,1024]{1,0:T(8,128)(2,1)}, bf16[1024,1024]{1,0:T(8,128)(2,1)S(1)}, u32[]{:S(2)}) copy-start(bf16[1024,1024]{1,0:T(8,128)(2,1)S(1)} %collective-permute-done.13.right) | copy-start | bytes 6291460
  33.2 1.3 copy-start.4
  33.3 44.9 %collective-permute-start.15 = (bf16[512,1024]{1,0:T(8,128)(2,1)S(1)}, bf16[512,1024]{1,0:T(8,128)(2,1)S(1)}, u32[]{:S(2)}, u32[]{:S(2)}) collective-permute-start(bf16[512,1024]{1,0:T(8,128)(2,1)S(1)} %slice.24), channel_id=1, source_target_pairs={{2,4},{11,13},{20,22},{29,31},{38,32},{47,41},{48,50},{57,59},{66,... | collective-permute-start | bytes 3145736 | tf_op jit(solution)/shard_map/ppermute | solution.py:281
  34.6 43.6 %collective-permute-start.16 = (bf16[512,1024]{1,0:T(8,128)(2,1)S(1)}, bf16[512,1024]{1,0:T(8,128)(2,1)}, u32[]{:S(2)}, u32[]{:S(2)}) collective-permute-start(bf16[512,1024]{1,0:T(8,128)(2,1)S(1)} %slice.25), channel_id=1, source_target_pairs={{6,4},{15,13},{16,22},{25,31},{34,32},{43,41},{52,50},{61,59},{70,... | collective-permute-start | bytes 3145736 | tf_op jit(solution)/shard_map/ppermute | solution.py:282
  36.8 6.7 %collective-permute-start.1 = (bf16[136,1024]{1,0:T(8,128)(2,1)S(1)}, bf16[136,1024]{1,0:T(8,128)(2,1)}, u32[]{:S(2)}, u32[]{:S(2)}) collective-permute-start(bf16[136,1024]{1,0:T(8,128)(2,1)S(1)} %copy-done.5), channel_id=1, source_target_pairs={{0,32},{32,64},{64,96},{96,128},{128,160},{160,192},{192,224},{224... | collective-permute-start | bytes 835592 | tf_op jit(solution)/shard_map/ppermute | solution.py:222
  36.8 9.7 %collective-permute-start.2 = (bf16[136,1024]{1,0:T(8,128)(2,1)S(1)}, bf16[136,1024]{1,0:T(8,128)(2,1)}, u32[]{:S(2)}, u32[]{:S(2)}) collective-permute-start(bf16[136,1024]{1,0:T(8,128)(2,1)S(1)} %copy-done.5), channel_id=1, source_target_pairs={{0,224},{32,0},{64,32},{96,64},{128,96},{160,128},{192,160},{224,1... | collective-permute-start | bytes 835592 | tf_op jit(solution)/shard_map/ppermute | solution.py:222
  43.5 10.6 %collective-permute-start.3 = (bf16[136,1024]{1,0:T(8,128)(2,1)}, bf16[136,1024]{1,0:T(8,128)(2,1)}, u32[]{:S(2)}, u32[]{:S(2)}) collective-permute-start(bf16[136,1024]{1,0:T(8,128)(2,1)} %collective-permute-done.1.refs_1_), channel_id=1, source_target_pairs={{0,32},{32,64},{64,96},{96,128},{128,160},{160,192},{192,224},{224... | collective-permute-start | bytes 835592 | tf_op jit(solution)/shard_map/ppermute | solution.py:222
  46.5 10.9 %collective-permute-start.6 = (bf16[136,1024]{1,0:T(8,128)(2,1)}, bf16[136,1024]{1,0:T(8,128)(2,1)}, u32[]{:S(2)}, u32[]{:S(2)}) collective-permute-start(bf16[136,1024]{1,0:T(8,128)(2,1)} %collective-permute-done.2.refs_2_), channel_id=1, source_target_pairs={{0,224},{32,0},{64,32},{96,64},{128,96},{160,128},{192,160},{224,1... | collective-permute-start | bytes 835592 | tf_op jit(solution)/shard_map/ppermute | solution.py:222
  49.7 37.4 %all-to-all-start = ((bf16[4,2,4,192,128]{4,3,2,1,0:T(8,128)(2,1)}), bf16[4,2,4,192,128]{4,3,2,1,0:T(8,128)(2,1)}, u32[]{:S(2)}, u32[]{:S(2)}) async-start(bf16[4,2,4,192,128]{4,3,2,1,0:T(8,128)(2,1)} %shard_map.74), calls=%async_computation | async-start | bytes 3145728 | tf_op jit(solution)/shard_map/all_to_all | solution.py:308
  54.1 9.1 %collective-permute-start.7 = (bf16[136,1024]{1,0:T(8,128)(2,1)}, bf16[136,1024]{1,0:T(8,128)(2,1)S(1)}, u32[]{:S(2)}, u32[]{:S(2)}) collective-permute-start(bf16[136,1024]{1,0:T(8,128)(2,1)} %collective-permute-done.3.refs_3_), channel_id=1, source_target_pairs={{0,32},{32,64},{64,96},{96,128},{128,160},{160,192},{192,224},{224... | collective-permute-start | bytes 835592 | tf_op jit(solution)/shard_map/ppermute | solution.py:222
  57.4 9.7 %collective-permute-start.8 = (bf16[136,1024]{1,0:T(8,128)(2,1)}, bf16[136,1024]{1,0:T(8,128)(2,1)S(1)}, u32[]{:S(2)}, u32[]{:S(2)}) collective-permute-start(bf16[136,1024]{1,0:T(8,128)(2,1)} %collective-permute-done.6.refs_0_), channel_id=1, source_target_pairs={{0,224},{32,0},{64,32},{96,64},{128,96},{160,128},{192,160},{224,1... | collective-permute-start | bytes 835592 | tf_op jit(solution)/shard_map/ppermute | solution.py:222
  63.2 12.0 %copy-start.7 = (bf16[136,1024]{1,0:T(8,128)(2,1)}, bf16[136,1024]{1,0:T(8,128)(2,1)S(1)}, u32[]{:S(2)}) copy-start(bf16[136,1024]{1,0:T(8,128)(2,1)S(1)} %collective-permute-done.7.refs_1_) | copy-start | bytes 835588
  63.9 11.3 %collective-permute-start.9 = (bf16[72,1024]{1,0:T(8,128)(2,1)}, bf16[72,1024]{1,0:T(8,128)(2,1)}, u32[]{:S(2)}, u32[]{:S(2)}) collective-permute-start(bf16[72,1024]{1,0:T(8,128)(2,1)} %slice.28), channel_id=1, source_target_pairs={{0,32},{32,64},{64,96},{96,128},{128,160},{160,192},{192,224},{224... | collective-permute-start | bytes 442376 | tf_op jit(solution)/shard_map/ppermute | solution.py:222
  67.1 0.7 copy-start.8
  68.5 6.7 %collective-permute-start.10 = (bf16[64,1024]{1,0:T(8,128)(2,1)}, bf16[64,1024]{1,0:T(8,128)(2,1)S(1)}, u32[]{:S(2)}, u32[]{:S(2)}) collective-permute-start(bf16[64,1024]{1,0:T(8,128)(2,1)} %slice.29), channel_id=1, source_target_pairs={{0,224},{32,0},{64,32},{96,64},{128,96},{160,128},{192,160},{224,1... | collective-permute-start | bytes 393224 | tf_op jit(solution)/shard_map/ppermute | solution.py:222
  75.2 0.7 copy-start.9
  78.2 1.0 copy-start.6
  82.1 41.6 %collective-permute-start.17 = (bf16[1024,1024]{1,0:T(8,128)(2,1)}, bf16[1024,1024]{1,0:T(8,128)(2,1)}, u32[]{:S(2)}, u32[]{:S(2)}) collective-permute-start(bf16[1024,1024]{1,0:T(8,128)(2,1)} %shard_map.77), channel_id=1, source_target_pairs={{0,1},{2,3},{4,5},{6,7},{9,8},{11,10},{13,12},{15,14},{16,17},{18,... | collective-permute-start | bytes 6291464 | tf_op jit(solution)/shard_map/ppermute | solution.py:288
  87.1 5.0 %copy-start = (bf16[544,1024]{1,0:T(8,128)(2,1)S(1)}, bf16[544,1024]{1,0:T(8,128)(2,1)}, u32[]{:S(2)}) copy-start(bf16[544,1024]{1,0:T(8,128)(2,1)} %shard_map.76.refs_1_) | copy-start | bytes 3342340
  87.1 8.0 %copy-start.1 = (bf16[544,1024]{1,0:T(8,128)(2,1)S(1)}, bf16[544,1024]{1,0:T(8,128)(2,1)}, u32[]{:S(2)}) copy-start(bf16[544,1024]{1,0:T(8,128)(2,1)} %shard_map.75.refs_0_) | copy-start | bytes 3342340
  87.1 28.8 %collective-permute-start.4 = (bf16[544,1024]{1,0:T(8,128)(2,1)}, bf16[544,1024]{1,0:T(8,128)(2,1)S(1)}, u32[]{:S(2)}, u32[]{:S(2)}) collective-permute-start(bf16[544,1024]{1,0:T(8,128)(2,1)} %shard_map.75.refs_0_), channel_id=1, source_target_pairs={{0,8},{8,16},{16,24},{24,0},{1,9},{9,17},{17,25},{25,1},{2,10},{10... | collective-permute-start | bytes 3342344 | tf_op jit(solution)/shard_map/ppermute | solution.py:222
  88.7 27.1 %collective-permute-start = (bf16[4,4,192,128]{3,2,1,0:T(8,128)(2,1)S(1)}, bf16[4,4,192,128]{3,2,1,0:T(8,128)(2,1)S(1)}, u32[]{:S(2)}, u32[]{:S(2)}) collective-permute-start(bf16[4,4,192,128]{3,2,1,0:T(8,128)(2,1)S(1)} %select_bitcast_fusion), channel_id=1, source_target_pairs={{0,32},{32,0},{1,33},{33,1},{2,34},{34,2},{3,35},{35,3},{4,36},{36... | collective-permute-start | bytes 2359304 | tf_op jit(solution)/shard_map/ppermute | solution.py:222
  92.0 28.7 %collective-permute-start.11 = (bf16[544,1024]{1,0:T(8,128)(2,1)S(1)}, bf16[544,1024]{1,0:T(8,128)(2,1)S(1)}, u32[]{:S(2)}, u32[]{:S(2)}) collective-permute-start(bf16[544,1024]{1,0:T(8,128)(2,1)S(1)} %copy-done), channel_id=1, source_target_pairs={{0,24},{8,0},{16,8},{24,16},{1,25},{9,1},{17,9},{25,17},{2,26},{10... | collective-permute-start | bytes 3342344 | tf_op jit(solution)/shard_map/ppermute | solution.py:222
  95.1 49.6 %collective-permute-start.18 = (bf16[544,1024]{1,0:T(8,128)(2,1)S(1)}, bf16[544,1024]{1,0:T(8,128)(2,1)S(1)}, u32[]{:S(2)}, u32[]{:S(2)}) collective-permute-start(bf16[544,1024]{1,0:T(8,128)(2,1)S(1)} %copy-done.1), channel_id=1, source_target_pairs={{0,24},{8,0},{16,8},{24,16},{1,25},{9,1},{17,9},{25,17},{2,26},{10... | collective-permute-start | bytes 3342344 | tf_op jit(solution)/shard_map/ppermute | solution.py:222
  115.9 28.8 %collective-permute-start.19 = (bf16[544,1024]{1,0:T(8,128)(2,1)S(1)}, bf16[544,1024]{1,0:T(8,128)(2,1)S(1)}, u32[]{:S(2)}, u32[]{:S(2)}) collective-permute-start(bf16[544,1024]{1,0:T(8,128)(2,1)S(1)} %copy-done), channel_id=1, source_target_pairs={{0,8},{8,16},{16,24},{24,0},{1,9},{9,17},{17,25},{25,1},{2,10},{10... | collective-permute-start | bytes 3342344 | tf_op jit(solution)/shard_map/ppermute | solution.py:222
  115.9 53.0 %collective-permute-start.5 = (bf16[544,1024]{1,0:T(8,128)(2,1)S(1)}, bf16[544,1024]{1,0:T(8,128)(2,1)S(1)}, u32[]{:S(2)}, u32[]{:S(2)}) collective-permute-start(bf16[544,1024]{1,0:T(8,128)(2,1)S(1)} %collective-permute-done.4.refs_2_), channel_id=1, source_target_pairs={{0,8},{8,16},{16,24},{24,0},{1,9},{9,17},{17,25},{25,1},{2,10},{10... | collective-permute-start | bytes 3342344 | tf_op jit(solution)/shard_map/ppermute | solution.py:222
  117.4 6.4 %copy-start.2 = (bf16[1024,1024]{1,0:T(8,128)(2,1)S(1)}, bf16[1024,1024]{1,0:T(8,128)(2,1)}, u32[]{:S(2)}) copy-start(bf16[1024,1024]{1,0:T(8,128)(2,1)} %shard_map.77) | copy-start | bytes 6291460
  120.8 48.1 %collective-permute-start.12 = (bf16[544,1024]{1,0:T(8,128)(2,1)S(1)}, bf16[544,1024]{1,0:T(8,128)(2,1)S(1)}, u32[]{:S(2)}, u32[]{:S(2)}) collective-permute-start(bf16[544,1024]{1,0:T(8,128)(2,1)S(1)} %collective-permute-done.11.refs_5_), channel_id=1, source_target_pairs={{0,24},{8,0},{16,8},{24,16},{1,25},{9,1},{17,9},{25,17},{2,26},{10... | collective-permute-start | bytes 3342344 | tf_op jit(solution)/shard_map/ppermute | solution.py:222
